TPU v7x, 32 devices: a whole 2x2x4 slice. The times are simulated.
32 devices in a mesh: kv: 8 (over z, y), tp: 4 (over x, core).
Axes of the slice: x: 2, y: 2, z: 4, core: 2. Of those that a mesh axis runs over, the one named last changes fastest.
Arguments:
- tokens: bfloat16 [4096, 2048], P('kv'), may hold values from -18 to 18
- w_query: bfloat16 [2048, 1024], P(None, 'tp'), may hold values from -0.125 to 0.125
- w_key: bfloat16 [2048, 256], P(None, 'tp'), may hold values from -0.125 to 0.125
- w_value: bfloat16 [2048, 256], P(None, 'tp'), may hold values from -18 to 18
- w_out: bfloat16 [1024, 2048], P(None, 'tp'), may hold values from -0.1875 to 0.1875
- out_gain: float32 [1024], replicated, may hold values from 0.1 to 1.9
- chosen: int32 [4, 64, 8], P('tp', 'kv'), may hold values from -1 to 63, as said below
Outputs:
- mixed_out: bfloat16 [4096, 2048], P('kv', 'tp')
Inputs may be any that keep to these rules, and one draw needn't show every extreme that they name: chosen[h, b, 0] is b itself; the other entries of a row are distinct key blocks lying wholly before block b, or -1, placed after all named blocks; for each key head h, the query blocks on one index of kv (its 512 positions) name, together, at most one key block of head h held by any other index of kv.
All inputs are finite; a program needn't handle non-finite values.
Results may differ from a plain program's by a relative error of at most 0.024.
Values may be sent and summed in bfloat16 or wider, within the bound.
No kernel may reach another device: no remote copies, remote signals or barrier semaphores. Data moves between devices by JAX's collectives and lax.ppermute only.
A program may use at most 64 MiB of HBM per device.

v0:
```python
import functools

import jax
import jax.numpy as jnp
import numpy as np
from jax import lax
from jax.experimental import pallas as pl
from jax.experimental.pallas import tpu as pltpu
from jax.sharding import PartitionSpec as P


HD = 64
BLK = 64
LANES = 2 * HD
PAIR = 2 * BLK
CHUNKS = 2
SIGN_FLOPS = 10**10
ROPE_BASE = 500000.0
NORM_EPS = 1e-06
MASKED = -1e30
F32 = jnp.float32
BF16 = jnp.bfloat16


def rope_tables(rows, places):
    half = HD // 2
    frequency = ROPE_BASE ** (-np.arange(half, dtype=np.float64) / half)
    reps = LANES // half

    def both(positions):
        angles = positions[:, None].astype(np.float64) * frequency[None, :]
        wide = np.tile(angles, (1, reps))
        return np.cos(wide).astype(np.float32), np.sin(wide).astype(np.float32)

    row_cos, row_sin = both(np.arange(rows))
    place_cos, place_sin = both(np.arange(places) * rows)
    return row_cos, row_sin, np.concatenate([place_cos, place_sin], axis=1)


def vmem():
    return pl.BlockSpec(memory_space=pltpu.VMEM)


def call(kernel, outs, n_in, flops, scratch=(), mib=16):
    return pl.pallas_call(
        kernel,
        out_shape=outs,
        in_specs=[vmem()] * n_in,
        out_specs=jax.tree.map(lambda _: vmem(), outs),
        scratch_shapes=list(scratch),
        compiler_params=pltpu.CompilerParams(vmem_limit_bytes=mib * 2**20),
        cost_estimate=pl.CostEstimate(flops=flops, bytes_accessed=2**20, transcendentals=0),
    )


def lane_index(shape):
    return lax.broadcasted_iota(jnp.int32, shape, len(shape) - 1)


def cos_sin(cos_ref, sin_ref, place_ref, sign_ref):
    place = place_ref[pl.ds(lax.axis_index("kv"), 1), :]
    pc, ps = place[:, :LANES], place[:, LANES:]
    rc, rs = cos_ref[...], sin_ref[...]
    cosine = rc * pc - rs * ps
    sine = rs * pc + rc * ps
    return cosine, sine * sign_ref[0:1, :]


def turn(values, cosine, sine):
    first = lane_index(values.shape) % HD < HD // 2
    swapped = jnp.where(
        first, pltpu.roll(values, LANES - HD // 2, 1), pltpu.roll(values, HD // 2, 1)
    )
    return values * cosine + swapped * sine


def sign_kernel(out_ref):
    first = lane_index(out_ref.shape) % HD < HD // 2
    out_ref[...] = jnp.where(first, -1.0, 1.0)


def qkv_kernel(
    x_ref, wk_ref, wv_ref, wq_ref, cos_ref, sin_ref, place_ref, sign_ref, pair_ref, q_ref, wkv_ref
):
    wkv_ref[:HD, :] = wk_ref[...]
    wkv_ref[HD:, :] = wv_ref[...]
    both = lax.dot_general(
        x_ref[...], wkv_ref[...], (((1,), (1,)), ((), ())), preferred_element_type=F32
    )
    cosine, sine = cos_sin(cos_ref, sin_ref, place_ref, sign_ref)
    turned = turn(both, cosine, sine)
    pair_ref[...] = jnp.where(lane_index(both.shape) < HD, turned, both).astype(BF16)
    q = jnp.dot(x_ref[...], wq_ref[...], preferred_element_type=F32)
    for j in range(q_ref.shape[1] // LANES):
        lanes = slice(j * LANES, (j + 1) * LANES)
        q_ref[:, lanes] = (turn(q[:, lanes], cosine, sine) * HD**-0.5).astype(BF16)


def pick_kernel(masks, *refs):
    *table_refs, pair_ref, out_ref = refs
    blocks = pair_ref.shape[0] // BLK
    me = lax.axis_index("kv")
    first = me * blocks

    def one(peer, table):
        local = table - first
        mine = (local >= 0) & (local < blocks)
        index = jnp.max(jnp.where(mine, local, 0))
        out_ref[peer] = pair_ref[pl.ds(pl.multiple_of(index * BLK, BLK), BLK), :]

    if masks:
        out_ref[me] = pair_ref[:BLK, :]
        for ref, group in zip(table_refs, masks, strict=True):
            for i, mask in enumerate(group):
                one(me ^ mask, ref[i])
    else:
        pl.loop(0, out_ref.shape[0])(lambda peer: one(peer, table_refs[0][peer]))


def heads_of(q, count):
    order = list(range(0, count, 2)) + list(range(1, count, 2))
    return jnp.concatenate([q[:, h * HD : (h + 1) * HD] for h in order], axis=0)


def value_forms(pairs):
    low = lane_index(pairs.shape) < HD
    one = jnp.ones((), BF16)
    wide = pairs.astype(F32)
    even = jnp.where(low, pltpu.roll(wide, HD, 1), 1.0).astype(BF16)
    odd = jnp.where(low, one, pairs)
    return even, odd


def attend(q, keys, even, odd, bias, rows, heads):
    stacked = heads_of(q, heads)
    scores = lax.dot_general(stacked, keys, (((1,), (1,)), ((), ())), preferred_element_type=F32)
    width = scores.shape[1]
    scores = (scores.reshape(heads, rows, width) + bias[None]).reshape(heads * rows, width)
    peak = jnp.max(scores, axis=1, keepdims=True)
    weights = jnp.exp(scores - peak).astype(BF16)
    split = heads // 2 * rows
    even_out = jnp.dot(weights[:split], even, preferred_element_type=F32)
    odd_out = jnp.dot(weights[split:], odd, preferred_element_type=F32)
    low = lane_index((rows, LANES)) < HD
    results = []
    for j in range(heads // 2):
        e = even_out[j * rows : (j + 1) * rows]
        o = odd_out[j * rows : (j + 1) * rows]
        total = jnp.where(low, e, o)
        sums = pltpu.roll(jnp.where(low, o, e), HD, 1)
        tops = jnp.where(
            low, peak[j * rows : (j + 1) * rows], peak[split + j * rows : split + (j + 1) * rows]
        )
        results.append((total, sums, tops))
    return results


def local_kernel(q_ref, pair_ref, ch_ref, lse_ref, o_ref):
    rows, width = q_ref.shape
    heads = width // HD
    blocks = rows // BLK
    names = ch_ref[...]
    key_block = lane_index((blocks, rows)) // BLK + lax.axis_index("kv") * blocks
    named = names[:, 0:1] == key_block
    for s in range(1, names.shape[1]):
        named = named | (names[:, s : s + 1] == key_block)
    bias = jnp.where(named, 0.0, MASKED)
    pairs = pair_ref[...]
    even, odd = value_forms(pairs)
    for i in range(rows // PAIR):
        at, span = i * PAIR, (i + 1) * PAIR
        mask = jnp.concatenate(
            [
                jnp.broadcast_to(bias[2 * i + k : 2 * i + k + 1, :span], (BLK, span))
                for k in range(2)
            ],
            axis=0,
        )
        row = lax.broadcasted_iota(jnp.int32, (PAIR, span), 0) + at
        mask = jnp.where(lane_index((PAIR, span)) <= row, mask, MASKED)
        parts = attend(
            q_ref[at:span, :], pairs[:span, :HD], even[:span], odd[:span], mask, PAIR, heads
        )
        for j, (total, sums, tops) in enumerate(parts):
            lanes = slice(j * LANES, (j + 1) * LANES)
            lse_ref[at:span, lanes] = tops + jnp.log(sums)
            o_ref[at:span, lanes] = (total / sums).astype(BF16)


def remote_kernel(start, ch_ref, q_ref, lse_ref, arr_ref, o_ref, out_ref, seen_ref):
    rows, width = out_ref.shape
    heads = width // HD
    blocks = q_ref.shape[0] // BLK
    peers = arr_ref.shape[0] // BLK
    group = 8 if peers % 8 == 0 else peers
    span = group * BLK
    me = lax.axis_index("kv")
    names = ch_ref[...]
    owners = jnp.where(names >= 0, names // blocks, me)
    away = jnp.where(owners == me, -1, owners)
    out_ref[...] = o_ref[start : start + rows, :]
    if peers > group:
        seen_ref[...] = lse_ref[start : start + rows, :]

    def block(b, bias, keys):
        first = start + b * BLK
        even, odd = value_forms(keys)
        parts = attend(
            q_ref[first : first + BLK, :], keys[:, :HD], even, odd, bias, BLK, heads
        )
        for j, (total, sums, tops) in enumerate(parts):
            at = (slice(first, first + BLK), slice(j * LANES, (j + 1) * LANES))
            here = (slice(b * BLK, (b + 1) * BLK), at[1])
            lse = seen_ref[here] if peers > group else lse_ref[at]
            top = jnp.maximum(lse, tops)
            old = jnp.exp(lse - top)
            new = jnp.exp(tops - top)
            both = old + sums * new
            mixed = (out_ref[here].astype(F32) * old + total * new) / both
            out_ref[here] = mixed.astype(BF16)
            if peers > group:
                seen_ref[here] = top + jnp.log(both)

    def one_group(g):
        base = g * group
        key_peer = lane_index((blocks, span)) // BLK + base
        named = away[:, 0:1] == key_peer
        for s in range(1, names.shape[1]):
            named = named | (away[:, s : s + 1] == key_peer)
        bias = jnp.where(named, 0.0, MASKED)
        for b in range(rows // BLK):
            row = bias[start // BLK + b : start // BLK + b + 1]
            used = jnp.max(row) > -1.0

            @pl.when(used)
            def _():
                keys = arr_ref[pl.ds(pl.multiple_of(base * BLK, span), span), :]
                block(b, jnp.broadcast_to(row, (BLK, span)), keys)

    if peers == group:
        one_group(0)
    else:
        pl.loop(0, peers // group)(one_group)


def out_kernel(columns, masks, *refs):
    *part_refs, gain_ref, w_ref, out_ref = refs[: len(masks) + 2] + refs[-1:]
    me = lax.axis_index("tp")
    width = part_refs[0].shape[1]
    squares = 0.0
    product = 0.0
    for mask, ref in zip(masks, part_refs, strict=True):
        at = pl.multiple_of((me ^ mask) * width, width)
        att = ref[...].astype(F32)
        squares = squares + jnp.sum(att * att, axis=1, keepdims=True)
        scaled = (att * gain_ref[:, pl.ds(at, width)]).astype(BF16)
        product = product + jnp.dot(
            scaled, w_ref[pl.ds(at, width), :], preferred_element_type=F32
        )
    inverse = lax.rsqrt(squares / columns + NORM_EPS)
    out_ref[...] = (inverse * product).astype(BF16)


def per_device(tables, tokens, w_query, w_key, w_value, w_out, out_gain, chosen):
    peers = lax.axis_size("kv")
    ways = lax.axis_size("tp")
    rows, depth = tokens.shape
    width = w_query.shape[1]
    names = chosen[0]
    row_cos, row_sin, place = (jnp.asarray(t) for t in tables)
    swap = {}
    if peers <= 16 and peers & (peers - 1) == 0:
        swap = {m: [(i, i ^ m) for i in range(peers)] for m in range(1, peers)}
        beside = lax.ppermute(chosen, "kv", swap[1])
    else:
        table = jnp.broadcast_to(names[None], (peers, *names.shape))
        asked = [lax.all_to_all(table, "kv", 0, 0, tiled=True)]
        masks = ()
    sign = call(sign_kernel, jax.ShapeDtypeStruct((8, LANES), F32), 0, SIGN_FLOPS, mib=1)()
    pairs, q = call(
        qkv_kernel,
        (
            jax.ShapeDtypeStruct((rows, LANES), BF16),
            jax.ShapeDtypeStruct((rows, width), BF16),
        ),
        8,
        2 * rows * depth * (LANES + width),
        [pltpu.VMEM((LANES, depth), BF16)],
        mib=16,
    )(tokens, w_key.T, w_value.T, w_query, row_cos, row_sin, place, sign)
    if swap:
        beside, pairs, q = lax.optimization_barrier((beside, pairs, q))
        both = jnp.concatenate([chosen, beside], axis=0)
        asked = [beside] + [lax.ppermute(both, "kv", swap[m]) for m in range(2, peers, 2)]
        masks = ((1,),) + tuple((m, m ^ 1) for m in range(2, peers, 2))
    outgoing = call(
        functools.partial(pick_kernel, masks),
        jax.ShapeDtypeStruct((peers, BLK, LANES), BF16),
        len(asked) + 1,
        10**6,
        mib=4,
    )(*asked, pairs)
    arrived = lax.all_to_all(outgoing, "kv", 0, 0, tiled=True).reshape(peers * BLK, LANES)
    step = rows // CHUNKS
    lse, attended = call(
        local_kernel,
        (
            jax.ShapeDtypeStruct((rows, width), F32),
            jax.ShapeDtypeStruct((rows, width), BF16),
        ),
        3,
        2 * 10**9,
        mib=16,
    )(q, pairs, names)
    flips = [1 << i for i in reversed(range((ways - 1).bit_length()))]
    swaps = {m: [(i, i ^ m) for i in range(ways)] for m in flips}
    gain = out_gain[None, :]
    columns = gain.shape[1]
    cols = w_out.shape[1]
    sent = []
    for c in range(CHUNKS):
        mixed = call(
            functools.partial(remote_kernel, c * step),
            jax.ShapeDtypeStruct((step, width), BF16),
            5,
            10**8,
            [pltpu.VMEM((step, width) if peers > 8 else (8, LANES), F32)],
        )(names, q, lse, arrived, attended)
        sent.append([mixed, lax.ppermute(mixed, "tp", swaps[flips[0]])])
    result = None
    for c, held in enumerate(sent):
        masks = [0, flips[0]]
        for m in flips[1:]:
            more = []
            for h in held:
                more.append(lax.ppermute(h, "tp", swaps[m]))
            held = held + more
            masks = masks + [k ^ m for k in masks]
        extra = [] if result is None else [result]
        result = pl.pallas_call(
            functools.partial(out_kernel, columns, masks),
            out_shape=jax.ShapeDtypeStruct((rows, cols), BF16),
            grid=(1,),
            in_specs=[vmem()] * (len(held) + 2)
            + [pl.BlockSpec(memory_space=pl.ANY)] * len(extra),
            out_specs=pl.BlockSpec((step, cols), lambda i, c=c: (c, 0)),
            input_output_aliases={len(held) + 2: 0} if extra else {},
            compiler_params=pltpu.CompilerParams(vmem_limit_bytes=16 * 2**20),
            cost_estimate=pl.CostEstimate(
                flops=2 * step * columns * cols, bytes_accessed=2**20, transcendentals=0
            ),
        )(*held, gain, w_out, *extra)
    return result


def solution(mesh):
    def run(tokens, *rest):
        rows = tokens.shape[0] // mesh.shape["kv"]
        tables = rope_tables(rows, mesh.shape["kv"])

        def body(*args):
            return per_device(tables, *args)

        return jax.shard_map(
            body,
            mesh=mesh,
            in_specs=(
                P("kv", None),
                P(None, "tp"),
                P(None, "tp"),
                P(None, "tp"),
                P(None, "tp"),
                P(),
                P("tp", "kv", None),
            ),
            out_specs=P("kv", "tp"),
            check_vma=False,
        )(tokens, *rest)

    return run
```

profile of v0, /device:TPU:0, one launch (start us, length us, event | category | flops | bytes accessed | tf_op | source)
XLA Modules:
  0.0 36.4 jit_solution(16789250277540024631)
XLA Ops:
  0.0 3.1 %collective-permute-start = (s32[1,8,8]{2,1,0:T(8,128)}, s32[1,8,8]{2,1,0:T(8,128)S(1)}, u32[]{:S(2)}, u32[]{:S(2)}) collective-permute-start(s32[1,8,8]{2,1,0:T(8,128)} %param.16), channel_id=1, source_target_pairs={{0,4},{4,0},{8,12},{12,8},{16,20},{20,16},{24,28},{28,24},{1,5},{5... | collective-permute-start | bytes 776 | tf_op jit(solution)/shard_map/ppermute | solution.py:274
  3.1 0.0 copy-done.5
  3.2 1.6 %shard_map.101 = (bf16[512,128]{1,0:T(8,128)(2,1)S(1)}, bf16[512,256]{1,0:T(8,128)(2,1)S(1)}) custom-call(bf16[512,2048]{1,0:T(8,128)(2,1)S(1)} %copy-done.1, bf16[64,2048]{1,0:T(8,128)(2,1)S(1)} %bitcast.7, bf16[64,2048]{1,0:T(8,128)(2,1)S(1)} %bitcast.8, bf16[2048,256]{1,0:T(8,128)(2,1)S(1)} %copy-done.2, f32[512,128]{1,0:T(8,128)S(1)} %copy-done.6, ...), custom_call_target="tpu_custom_call" | custom-call | flops 805306368 | bytes 1048576 | tf_op jit(solution)/shard_map/pallas_call | solution.py:280
  4.8 0.1 collective-permute-done.refs_0_
  4.9 4.1 %collective-permute-start.3 = (s32[2,8,8]{2,1,0:T(8,128)S(1)}, s32[2,8,8]{2,1,0:T(8,128)S(1)}, u32[]{:S(2)}, u32[]{:S(2)}) collective-permute-start(s32[2,8,8]{2,1,0:T(8,128)S(1)} %constant_dynamic-update-slice_fusion), channel_id=1, source_target_pairs={{0,24},{4,28},{8,16},{12,20},{16,8},{20,12},{24,0},{28,4},{1,25},{... | collective-permute-start | bytes 1544 | tf_op jit(solution)/shard_map/ppermute | solution.py:294
  9.0 0.0 collective-permute-start.2
  9.0 0.6 %collective-permute-start.1 = (s32[2,8,8]{2,1,0:T(8,128)S(1)}, s32[2,8,8]{2,1,0:T(8,128)S(1)}, u32[]{:S(2)}, u32[]{:S(2)}) collective-permute-start(s32[2,8,8]{2,1,0:T(8,128)S(1)} %constant_dynamic-update-slice_fusion), channel_id=1, source_target_pairs={{0,8},{4,12},{8,0},{12,4},{16,24},{20,28},{24,16},{28,20},{1,9},{5... | collective-permute-start | bytes 1544 | tf_op jit(solution)/shard_map/ppermute | solution.py:294
  9.7 1.0 %collective-permute-done.3.refs_3_ = s32[2,8,8]{2,1,0:T(8,128)S(1)} collective-permute-done((s32[2,8,8]{2,1,0:T(8,128)S(1)}, s32[2,8,8]{2,1,0:T(8,128)S(1)}, u32[]{:S(2)}, u32[]{:S(2)}) %collective-permute-start.3) | collective-permute-done | bytes 544 | tf_op jit(solution)/shard_map/ppermute | solution.py:294
  10.7 2.9 %collective-permute-done.2.refs_2_ = s32[2,8,8]{2,1,0:T(8,128)S(1)} collective-permute-done((s32[2,8,8]{2,1,0:T(8,128)S(1)}, s32[2,8,8]{2,1,0:T(8,128)S(1)}, u32[]{:S(2)}, u32[]{:S(2)}) %collective-permute-start.2) | collective-permute-done | bytes 544 | tf_op jit(solution)/shard_map/ppermute | solution.py:294
  13.6 0.0 collective-permute-done.1.refs_1_
  13.6 0.9 %shard_map.103 = bf16[8,64,128]{2,1,0:T(8,128)(2,1)} custom-call(s32[1,8,8]{2,1,0:T(8,128)S(1)} %collective-permute-done.refs_0_, s32[2,8,8]{2,1,0:T(8,128)S(1)} %collective-permute-done.1.refs_1_, s32[2,8,8]{2,1,0:T(8,128)S(1)} %collective-permute-done.2.refs_2_, s32[2,8,8]{2,1,0:T(8,128)S(1)} %collective-permute-done.3.refs_3_, ...), custom_call_target="tpu_custom_call" | custom-call | flops 1000000 | bytes 1048576 | tf_op jit(solution)/shard_map/pallas_call | solution.py:296
  14.5 4.3 %all-to-all-start = ((bf16[8,64,128]{2,1,0:T(8,128)(2,1)}), bf16[8,64,128]{2,1,0:T(8,128)(2,1)S(1)}, u32[]{:S(2)}, u32[]{:S(2)}) async-start(bf16[8,64,128]{2,1,0:T(8,128)(2,1)} %shard_map.103), calls=%async_computation | async-start | bytes 262144 | tf_op jit(solution)/shard_map/all_to_all | solution.py:303
  18.7 1.7 %shard_map.102 = (f32[512,256]{1,0:T(8,128)S(1)}, bf16[512,256]{1,0:T(8,128)(2,1)S(1)}) custom-call(bf16[512,256]{1,0:T(8,128)(2,1)S(1)} %get-tuple-element.14.q_ref, bf16[512,128]{1,0:T(8,128)(2,1)S(1)} %get-tuple-element.15.pair_ref.refs_4_, s32[8,8]{1,0:T(8,128)S(1)} %bitcast.9), custom_call_target="tpu_custom_call" | custom-call | flops 2000000000 | bytes 1048576 | tf_op jit(solution)/shard_map/pallas_call | solution.py:305
  20.4 0.0 copy-start
  20.4 0.0 copy-start.8
  20.4 5.7 %all-to-all-done = bf16[8,64,128]{2,1,0:T(8,128)(2,1)S(1)} async-done(((bf16[8,64,128]{2,1,0:T(8,128)(2,1)}), bf16[8,64,128]{2,1,0:T(8,128)(2,1)S(1)}, u32[]{:S(2)}, u32[]{:S(2)}) %all-to-all-start) | async-done | bytes 131104 | tf_op jit(solution)/shard_map/all_to_all | solution.py:303
  26.1 0.6 %shard_map.105.refs_0_ = bf16[256,256]{1,0:T(8,128)(2,1)S(1)} custom-call(s32[8,8]{1,0:T(8,128)S(1)} %bitcast.10, bf16[512,256]{1,0:T(8,128)(2,1)S(1)} %get-tuple-element.14.q_ref, f32[512,256]{1,0:T(8,128)S(1)} %get-tuple-element.16.lse_ref, bf16[512,128]{1,0:T(8,128)(2,1)S(1)} %bitcast.5, bf16[512,256]{1,0:T(8,128)(2,1)S(1)} %get-tuple-element.18.o_ref), custom_call_target="tpu_custom_call" | custom-call | flops 100000000 | bytes 1048576 | tf_op jit(solution)/shard_map/pallas_call | solution.py:322
  26.7 1.6 %collective-permute-start.7 = (bf16[256,256]{1,0:T(8,128)(2,1)S(1)}, bf16[256,256]{1,0:T(8,128)(2,1)S(1)}, u32[]{:S(2)}, u32[]{:S(2)}) collective-permute-start(bf16[256,256]{1,0:T(8,128)(2,1)S(1)} %shard_map.105.refs_0_), channel_id=1, source_target_pairs={{0,2},{1,3},{2,0},{3,1},{4,6},{5,7},{6,4},{7,5},{8,10},{9,11},{10,... | collective-permute-start | bytes 393224 | tf_op jit(solution)/shard_map/ppermute | solution.py:329
  28.2 0.6 %shard_map.104.refs_0_ = bf16[256,256]{1,0:T(8,128)(2,1)S(1)} custom-call(s32[8,8]{1,0:T(8,128)S(1)} %bitcast.11, bf16[512,256]{1,0:T(8,128)(2,1)S(1)} %get-tuple-element.14.q_ref, f32[512,256]{1,0:T(8,128)S(1)} %get-tuple-element.16.lse_ref, bf16[512,128]{1,0:T(8,128)(2,1)S(1)} %bitcast.6, bf16[512,256]{1,0:T(8,128)(2,1)S(1)} %get-tuple-element.18.o_ref), custom_call_target="tpu_custom_call" | custom-call | flops 100000000 | bytes 1048576 | tf_op jit(solution)/shard_map/pallas_call | solution.py:322
  28.8 0.6 %collective-permute-start.4 = (bf16[256,256]{1,0:T(8,128)(2,1)S(1)}, bf16[256,256]{1,0:T(8,128)(2,1)S(1)}, u32[]{:S(2)}, u32[]{:S(2)}) collective-permute-start(bf16[256,256]{1,0:T(8,128)(2,1)S(1)} %shard_map.104.refs_0_), channel_id=1, source_target_pairs={{0,2},{1,3},{2,0},{3,1},{4,6},{5,7},{6,4},{7,5},{8,10},{9,11},{10,... | collective-permute-start | bytes 393224 | tf_op jit(solution)/shard_map/ppermute | solution.py:329
  29.4 0.0 collective-permute-start.8
  29.4 2.3 %collective-permute-done.7.refs_1_ = bf16[256,256]{1,0:T(8,128)(2,1)S(1)} collective-permute-done((bf16[256,256]{1,0:T(8,128)(2,1)S(1)}, bf16[256,256]{1,0:T(8,128)(2,1)S(1)}, u32[]{:S(2)}, u32[]{:S(2)}) %collective-permute-start.7) | collective-permute-done | bytes 131104 | tf_op jit(solution)/shard_map/ppermute | solution.py:329
  31.7 0.0 collective-permute-start.9
  31.7 0.5 %collective-permute-start.5 = (bf16[256,256]{1,0:T(8,128)(2,1)S(1)}, bf16[256,256]{1,0:T(8,128)(2,1)S(1)}, u32[]{:S(2)}, u32[]{:S(2)}) collective-permute-start(bf16[256,256]{1,0:T(8,128)(2,1)S(1)} %shard_map.104.refs_0_), channel_id=1, source_target_pairs={{0,1},{1,0},{2,3},{3,2},{4,5},{5,4},{6,7},{7,6},{8,9},{9,8},{10,11... | collective-permute-start | bytes 393224 | tf_op jit(solution)/shard_map/ppermute | solution.py:336
  32.2 1.6 %collective-permute-done.4.refs_1_ = bf16[256,256]{1,0:T(8,128)(2,1)S(1)} collective-permute-done((bf16[256,256]{1,0:T(8,128)(2,1)S(1)}, bf16[256,256]{1,0:T(8,128)(2,1)S(1)}, u32[]{:S(2)}, u32[]{:S(2)}) %collective-permute-start.4) | collective-permute-done | bytes 131104 | tf_op jit(solution)/shard_map/ppermute | solution.py:329
  33.8 0.0 collective-permute-start.6
  33.8 0.0 collective-permute-done.8.refs_2_
  33.9 0.0 collective-permute-done.9.refs_3_
  33.9 1.2 %shard_map.106.refs_6_ = bf16[512,512]{1,0:T(8,128)(2,1)} custom-call(bf16[256,256]{1,0:T(8,128)(2,1)S(1)} %shard_map.105.refs_0_, bf16[256,256]{1,0:T(8,128)(2,1)S(1)} %collective-permute-done.7.refs_1_, bf16[256,256]{1,0:T(8,128)(2,1)S(1)} %collective-permute-done.8.refs_2_, bf16[256,256]{1,0:T(8,128)(2,1)S(1)} %collective-permute-done.9.refs_3_, ...), custom_call_target="tpu_custom_call" | custom-call | flops 268435456 | bytes 1048576 | tf_op jit(solution)/shard_map/pallas_call | solution.py:340
  35.1 0.0 collective-permute-done.5.refs_2_
  35.1 0.1 collective-permute-done.6.refs_3_
  35.2 1.2 %shard_map.107 = bf16[512,512]{1,0:T(8,128)(2,1)} custom-call(bf16[256,256]{1,0:T(8,128)(2,1)S(1)} %shard_map.104.refs_0_, bf16[256,256]{1,0:T(8,128)(2,1)S(1)} %collective-permute-done.4.refs_1_, bf16[256,256]{1,0:T(8,128)(2,1)S(1)} %collective-permute-done.5.refs_2_, ...), custom_call_target="tpu_custom_call", output_to_operand_aliasing={{}: (6, {})} | custom-call | flops 268435456 | bytes 1048576 | tf_op jit(solution)/shard_map/pallas_call | solution.py:340
  (20 shorter events, 0.0 us)
Async XLA Ops:
  0.0 3.1 %copy-start.5 = (f32[512,128]{1,0:T(8,128)S(1)}, f32[512,128]{1,0:T(8,128)}, u32[]{:S(2)}) copy-start(f32[512,128]{1,0:T(8,128)} %constant.7.clone.sin_ref) | copy-start | bytes 786436
  0.0 3.1 %copy-start.6 = (f32[512,128]{1,0:T(8,128)S(1)}, f32[512,128]{1,0:T(8,128)}, u32[]{:S(2)}) copy-start(f32[512,128]{1,0:T(8,128)} %constant.6.clone.cos_ref) | copy-start | bytes 786436
  0.0 3.1 %copy-start.9 = (f32[8,256]{1,0:T(8,128)S(1)}, f32[8,256]{1,0:T(8,128)}, u32[]{:S(2)}) copy-start(f32[8,256]{1,0:T(8,128)} %constant.8.clone.place_ref) | copy-start | bytes 24580
  0.0 3.1 %copy-start.7 = (s32[1,8,8]{2,1,0:T(8,128)S(1)}, s32[1,8,8]{2,1,0:T(8,128)}, u32[]{:S(2)}) copy-start(s32[1,8,8]{2,1,0:T(8,128)} %param.16) | copy-start | bytes 772
  0.0 3.2 %copy-start.4 = (bf16[2048,64]{0,1:T(8,128)(2,1)S(1)}, bf16[2048,64]{0,1:T(8,128)(2,1)}, u32[]{:S(2)}) copy-start(bf16[2048,64]{0,1:T(8,128)(2,1)} %param.13) | copy-start | bytes 786436
  0.0 3.2 %copy-start.3 = (bf16[2048,64]{0,1:T(8,128)(2,1)S(1)}, bf16[2048,64]{0,1:T(8,128)(2,1)}, u32[]{:S(2)}) copy-start(bf16[2048,64]{0,1:T(8,128)(2,1)} %param.12) | copy-start | bytes 786436
  0.0 3.2 %copy-start.2 = (bf16[2048,256]{1,0:T(8,128)(2,1)S(1)}, bf16[2048,256]{1,0:T(8,128)(2,1)}, u32[]{:S(2)}) copy-start(bf16[2048,256]{1,0:T(8,128)(2,1)} %wq_ref.1) | copy-start | bytes 3145732
  0.0 3.2 %copy-start.1 = (bf16[512,2048]{1,0:T(8,128)(2,1)S(1)}, bf16[512,2048]{1,0:T(8,128)(2,1)}, u32[]{:S(2)}) copy-start(bf16[512,2048]{1,0:T(8,128)(2,1)} %x_ref.1) | copy-start | bytes 6291460
  0.0 4.9 %collective-permute-start = (s32[1,8,8]{2,1,0:T(8,128)}, s32[1,8,8]{2,1,0:T(8,128)S(1)}, u32[]{:S(2)}, u32[]{:S(2)}) collective-permute-start(s32[1,8,8]{2,1,0:T(8,128)} %param.16), channel_id=1, source_target_pairs={{0,4},{4,0},{8,12},{12,8},{16,20},{20,16},{24,28},{28,24},{1,5},{5... | collective-permute-start | bytes 776 | tf_op jit(solution)/shard_map/ppermute | solution.py:274
  4.9 5.8 %collective-permute-start.3 = (s32[2,8,8]{2,1,0:T(8,128)S(1)}, s32[2,8,8]{2,1,0:T(8,128)S(1)}, u32[]{:S(2)}, u32[]{:S(2)}) collective-permute-start(s32[2,8,8]{2,1,0:T(8,128)S(1)} %constant_dynamic-update-slice_fusion), channel_id=1, source_target_pairs={{0,24},{4,28},{8,16},{12,20},{16,8},{20,12},{24,0},{28,4},{1,25},{... | collective-permute-start | bytes 1544 | tf_op jit(solution)/shard_map/ppermute | solution.py:294
  9.0 4.5 %collective-permute-start.2 = (s32[2,8,8]{2,1,0:T(8,128)S(1)}, s32[2,8,8]{2,1,0:T(8,128)S(1)}, u32[]{:S(2)}, u32[]{:S(2)}) collective-permute-start(s32[2,8,8]{2,1,0:T(8,128)S(1)} %constant_dynamic-update-slice_fusion), channel_id=1, source_target_pairs={{0,16},{4,20},{8,24},{12,28},{16,0},{20,4},{24,8},{28,12},{1,17},{... | collective-permute-start | bytes 1544 | tf_op jit(solution)/shard_map/ppermute | solution.py:294
  9.0 4.5 %collective-permute-start.1 = (s32[2,8,8]{2,1,0:T(8,128)S(1)}, s32[2,8,8]{2,1,0:T(8,128)S(1)}, u32[]{:S(2)}, u32[]{:S(2)}) collective-permute-start(s32[2,8,8]{2,1,0:T(8,128)S(1)} %constant_dynamic-update-slice_fusion), channel_id=1, source_target_pairs={{0,8},{4,12},{8,0},{12,4},{16,24},{20,28},{24,16},{28,20},{1,9},{5... | collective-permute-start | bytes 1544 | tf_op jit(solution)/shard_map/ppermute | solution.py:294
  14.5 11.6 %all-to-all-start = ((bf16[8,64,128]{2,1,0:T(8,128)(2,1)}), bf16[8,64,128]{2,1,0:T(8,128)(2,1)S(1)}, u32[]{:S(2)}, u32[]{:S(2)}) async-start(bf16[8,64,128]{2,1,0:T(8,128)(2,1)} %shard_map.103), calls=%async_computation | async-start | bytes 262144 | tf_op jit(solution)/shard_map/all_to_all | solution.py:303
  20.4 13.5 %copy-start = (bf16[1024,512]{1,0:T(8,128)(2,1)S(1)}, bf16[1024,512]{1,0:T(8,128)(2,1)}, u32[]{:S(2)}) copy-start(bf16[1024,512]{1,0:T(8,128)(2,1)} %refs_5_.3) | copy-start | bytes 3145732
  20.4 13.5 %copy-start.8 = (f32[1024]{0:T(1024)S(1)}, f32[1024]{0:T(1024)}, u32[]{:S(2)}) copy-start(f32[1024]{0:T(1024)} %param.15) | copy-start | bytes 12292
  26.7 5.0 %collective-permute-start.7 = (bf16[256,256]{1,0:T(8,128)(2,1)S(1)}, bf16[256,256]{1,0:T(8,128)(2,1)S(1)}, u32[]{:S(2)}, u32[]{:S(2)}) collective-permute-start(bf16[256,256]{1,0:T(8,128)(2,1)S(1)} %shard_map.105.refs_0_), channel_id=1, source_target_pairs={{0,2},{1,3},{2,0},{3,1},{4,6},{5,7},{6,4},{7,5},{8,10},{9,11},{10,... | collective-permute-start | bytes 393224 | tf_op jit(solution)/shard_map/ppermute | solution.py:329
  28.8 5.0 %collective-permute-start.4 = (bf16[256,256]{1,0:T(8,128)(2,1)S(1)}, bf16[256,256]{1,0:T(8,128)(2,1)S(1)}, u32[]{:S(2)}, u32[]{:S(2)}) collective-permute-start(bf16[256,256]{1,0:T(8,128)(2,1)S(1)} %shard_map.104.refs_0_), channel_id=1, source_target_pairs={{0,2},{1,3},{2,0},{3,1},{4,6},{5,7},{6,4},{7,5},{8,10},{9,11},{10,... | collective-permute-start | bytes 393224 | tf_op jit(solution)/shard_map/ppermute | solution.py:329
  29.4 4.4 %collective-permute-start.8 = (bf16[256,256]{1,0:T(8,128)(2,1)S(1)}, bf16[256,256]{1,0:T(8,128)(2,1)S(1)}, u32[]{:S(2)}, u32[]{:S(2)}) collective-permute-start(bf16[256,256]{1,0:T(8,128)(2,1)S(1)} %shard_map.105.refs_0_), channel_id=1, source_target_pairs={{0,1},{1,0},{2,3},{3,2},{4,5},{5,4},{6,7},{7,6},{8,9},{9,8},{10,11... | collective-permute-start | bytes 393224 | tf_op jit(solution)/shard_map/ppermute | solution.py:336
  31.7 2.2 %collective-permute-start.9 = (bf16[256,256]{1,0:T(8,128)(2,1)S(1)}, bf16[256,256]{1,0:T(8,128)(2,1)S(1)}, u32[]{:S(2)}, u32[]{:S(2)}) collective-permute-start(bf16[256,256]{1,0:T(8,128)(2,1)S(1)} %collective-permute-done.7.refs_1_), channel_id=1, source_target_pairs={{0,1},{1,0},{2,3},{3,2},{4,5},{5,4},{6,7},{7,6},{8,9},{9,8},{10,11... | collective-permute-start | bytes 393224 | tf_op jit(solution)/shard_map/ppermute | solution.py:336
  31.7 3.4 %collective-permute-start.5 = (bf16[256,256]{1,0:T(8,128)(2,1)S(1)}, bf16[256,256]{1,0:T(8,128)(2,1)S(1)}, u32[]{:S(2)}, u32[]{:S(2)}) collective-permute-start(bf16[256,256]{1,0:T(8,128)(2,1)S(1)} %shard_map.104.refs_0_), channel_id=1, source_target_pairs={{0,1},{1,0},{2,3},{3,2},{4,5},{5,4},{6,7},{7,6},{8,9},{9,8},{10,11... | collective-permute-start | bytes 393224 | tf_op jit(solution)/shard_map/ppermute | solution.py:336
  33.8 1.3 %collective-permute-start.6 = (bf16[256,256]{1,0:T(8,128)(2,1)S(1)}, bf16[256,256]{1,0:T(8,128)(2,1)S(1)}, u32[]{:S(2)}, u32[]{:S(2)}) collective-permute-start(bf16[256,256]{1,0:T(8,128)(2,1)S(1)} %collective-permute-done.4.refs_1_), channel_id=1, source_target_pairs={{0,1},{1,0},{2,3},{3,2},{4,5},{5,4},{6,7},{7,6},{8,9},{9,8},{10,11... | collective-permute-start | bytes 393224 | tf_op jit(solution)/shard_map/ppermute | solution.py:336
where the time goes:
time: 36.6 us; the launch traced here: 36.4 us
  starting transfers between devices  14.8 us (40%)
  waiting for transfers between devices  13.7 us (37%)
  Pallas kernels  7.66 us (21%)
    all_to_all x1, waiting for transfers between devices, per_device(): lax.all_to_all(outgoing, 'kv', 0, 0, tiled=True).reshape(peers * BLK, LANES)  5.66 us
    ppermute x3, starting transfers between devices, per_device(): lax.ppermute(both, 'kv', swap[m])  4.76 us
    all_to_all x1, starting transfers between devices, per_device(): lax.all_to_all(outgoing, 'kv', 0, 0, tiled=True).reshape(peers * BLK, LANES)  4.25 us
    ppermute x2, waiting for transfers between devices, per_device(): sent.append([mixed, lax.ppermute(mixed, 'tp', swaps[flips[0]])])  3.92 us
    ppermute x3, waiting for transfers between devices, per_device(): lax.ppermute(both, 'kv', swap[m])  3.91 us
    ppermute x1, starting transfers between devices, per_device(): beside = lax.ppermute(chosen, 'kv', swap[1])  3.08 us
    pallas_call x2, Pallas kernels, per_device(): pl.pallas_call(functools.partial(out_kernel, columns, masks), out_shape=j...  2.37 us
    ppermute x2, starting transfers between devices, per_device(): sent.append([mixed, lax.ppermute(mixed, 'tp', swaps[flips[0]])])  2.16 us
  transfers between devices with their start and end apart: 11, of which 7 were waited for; matrix products, arithmetic and copies ran while one was open for 0% of the time, Pallas kernels for 14%

commit v1 on v0

--- a/solution.py
+++ b/solution.py
@@ -268,15 +268,19 @@
     width = w_query.shape[1]
     names = chosen[0]
     row_cos, row_sin, place = (jnp.asarray(t) for t in tables)
-    swap = {}
-    if peers <= 16 and peers & (peers - 1) == 0:
+    sign = call(sign_kernel, jax.ShapeDtypeStruct((8, LANES), F32), 0, SIGN_FLOPS, mib=1)()
+    if spread(peers):
         swap = {m: [(i, i ^ m) for i in range(peers)] for m in range(1, peers)}
         beside = lax.ppermute(chosen, "kv", swap[1])
+        both = jnp.concatenate([chosen, beside], axis=0)
+        asked, masks = [beside], [(1,)]
+        for m in range(peers - 2, 0, -2):
+            asked.append(lax.ppermute(both, "kv", swap[m]))
+            masks.append((m, m ^ 1))
     else:
         table = jnp.broadcast_to(names[None], (peers, *names.shape))
         asked = [lax.all_to_all(table, "kv", 0, 0, tiled=True)]
-        masks = ()
-    sign = call(sign_kernel, jax.ShapeDtypeStruct((8, LANES), F32), 0, SIGN_FLOPS, mib=1)()
+        masks = []
     pairs, q = call(
         qkv_kernel,
         (
@@ -288,11 +292,6 @@
         [pltpu.VMEM((LANES, depth), BF16)],
         mib=16,
     )(tokens, w_key.T, w_value.T, w_query, row_cos, row_sin, place, sign)
-    if swap:
-        beside, pairs, q = lax.optimization_barrier((beside, pairs, q))
-        both = jnp.concatenate([chosen, beside], axis=0)
-        asked = [beside] + [lax.ppermute(both, "kv", swap[m]) for m in range(2, peers, 2)]
-        masks = ((1,),) + tuple((m, m ^ 1) for m in range(2, peers, 2))
     outgoing = call(
         functools.partial(pick_kernel, masks),
         jax.ShapeDtypeStruct((peers, BLK, LANES), BF16),
@@ -318,7 +317,7 @@
     columns = gain.shape[1]
     cols = w_out.shape[1]
     sent = []
-    for c in range(CHUNKS):
+    for c in reversed(range(CHUNKS)):
         mixed = call(
             functools.partial(remote_kernel, c * step),
             jax.ShapeDtypeStruct((step, width), BF16),
@@ -326,9 +325,9 @@
             10**8,
             [pltpu.VMEM((step, width) if peers > 8 else (8, LANES), F32)],
         )(names, q, lse, arrived, attended)
-        sent.append([mixed, lax.ppermute(mixed, "tp", swaps[flips[0]])])
+        sent.append((c, [mixed, lax.ppermute(mixed, "tp", swaps[flips[0]])]))
     result = None
-    for c, held in enumerate(sent):
+    for c, held in sent:
         masks = [0, flips[0]]
         for m in flips[1:]:
             more = []
@@ -353,6 +352,10 @@
     return result
 
 
+def spread(peers):
+    return peers <= 16 and peers & (peers - 1) == 0
+
+
 def solution(mesh):
     def run(tokens, *rest):
         rows = tokens.shape[0] // mesh.shape["kv"]

time: 36.6 us -> 37.1 us (1.014)
  waiting for transfers between devices: 13.7 us -> 15.2 us
  starting transfers between devices: 14.8 us -> 13.8 us
    ppermute x1, waiting for transfers between devices: 0.12 us -> 1.79 us  [per_device(): beside = lax.ppermute(chosen, 'kv', swap[1])]
    all_to_all x1, starting transfers between devices: 4.25 us -> 3.37 us  [per_device(): lax.all_to_all(outgoing, 'kv', 0, 0, tiled=True).reshape(peers * BLK, LANES)]
where the time goes in v1:
time: 37.1 us; the launch traced here: 36.9 us
  waiting for transfers between devices  15.2 us (41%)
  starting transfers between devices  13.8 us (37%)
  Pallas kernels  7.66 us (21%)
    all_to_all x1, waiting for transfers between devices, per_device(): lax.all_to_all(outgoing, 'kv', 0, 0, tiled=True).reshape(peers * BLK, LANES)  5.59 us
    ppermute x3, starting transfers between devices, per_device(): asked.append(lax.ppermute(both, 'kv', swap[m]))  4.67 us
    ppermute x2, waiting for transfers between devices, per_device(): sent.append((c, [mixed, lax.ppermute(mixed, 'tp', swaps[flips[0]])]))  3.92 us
    ppermute x3, waiting for transfers between devices, per_device(): asked.append(lax.ppermute(both, 'kv', swap[m]))  3.79 us
    all_to_all x1, starting transfers between devices, per_device(): lax.all_to_all(outgoing, 'kv', 0, 0, tiled=True).reshape(peers * BLK, LANES)  3.37 us
    ppermute x1, starting transfers between devices, per_device(): beside = lax.ppermute(chosen, 'kv', swap[1])  3.08 us
    pallas_call x2, Pallas kernels, per_device(): pl.pallas_call(functools.partial(out_kernel, columns, masks), out_shape=j...  2.37 us
    ppermute x2, starting transfers between devices, per_device(): sent.append((c, [mixed, lax.ppermute(mixed, 'tp', swaps[flips[0]])]))  2.16 us
  transfers between devices with their start and end apart: 11, of which 7 were waited for; matrix products, arithmetic and copies ran while one was open for 0% of the time, Pallas kernels for 14%

profile of v1, /device:TPU:0, one launch (start us, length us, event | category | flops | bytes accessed | tf_op | source)
XLA Modules:
  0.0 36.9 jit_solution(7253136118962521603)
XLA Ops:
  0.0 3.1 %collective-permute-start = (s32[1,8,8]{2,1,0:T(8,128)}, s32[1,8,8]{2,1,0:T(8,128)S(1)}, u32[]{:S(2)}, u32[]{:S(2)}) collective-permute-start(s32[1,8,8]{2,1,0:T(8,128)} %param.16), channel_id=1, source_target_pairs={{0,4},{4,0},{8,12},{12,8},{16,20},{20,16},{24,28},{28,24},{1,5},{5... | collective-permute-start | bytes 776 | tf_op jit(solution)/shard_map/ppermute | solution.py:274
  3.1 1.8 %collective-permute-done.refs_0_ = s32[1,8,8]{2,1,0:T(8,128)S(1)} collective-permute-done((s32[1,8,8]{2,1,0:T(8,128)}, s32[1,8,8]{2,1,0:T(8,128)S(1)}, u32[]{:S(2)}, u32[]{:S(2)}) %collective-permute-start) | collective-permute-done | bytes 288 | tf_op jit(solution)/shard_map/ppermute | solution.py:274
  4.9 2.1 %collective-permute-start.3 = (s32[2,8,8]{2,1,0:T(8,128)S(1)}, s32[2,8,8]{2,1,0:T(8,128)S(1)}, u32[]{:S(2)}, u32[]{:S(2)}) collective-permute-start(s32[2,8,8]{2,1,0:T(8,128)S(1)} %constant_dynamic-update-slice_fusion), channel_id=1, source_target_pairs={{0,8},{4,12},{8,0},{12,4},{16,24},{20,28},{24,16},{28,20},{1,9},{5... | collective-permute-start | bytes 1544 | tf_op jit(solution)/shard_map/ppermute | solution.py:278
  7.0 2.6 %collective-permute-start.2 = (s32[2,8,8]{2,1,0:T(8,128)S(1)}, s32[2,8,8]{2,1,0:T(8,128)S(1)}, u32[]{:S(2)}, u32[]{:S(2)}) collective-permute-start(s32[2,8,8]{2,1,0:T(8,128)S(1)} %constant_dynamic-update-slice_fusion), channel_id=1, source_target_pairs={{0,16},{4,20},{8,24},{12,28},{16,0},{20,4},{24,8},{28,12},{1,17},{... | collective-permute-start | bytes 1544 | tf_op jit(solution)/shard_map/ppermute | solution.py:278
  9.6 0.0 collective-permute-start.1
  9.6 0.0 copy-done.5
  9.6 1.6 %shard_map.101 = (bf16[512,128]{1,0:T(8,128)(2,1)S(1)}, bf16[512,256]{1,0:T(8,128)(2,1)S(1)}) custom-call(bf16[512,2048]{1,0:T(8,128)(2,1)S(1)} %copy-done.1, bf16[64,2048]{1,0:T(8,128)(2,1)S(1)} %bitcast.7, bf16[64,2048]{1,0:T(8,128)(2,1)S(1)} %bitcast.8, bf16[2048,256]{1,0:T(8,128)(2,1)S(1)} %copy-done.2, f32[512,128]{1,0:T(8,128)S(1)} %copy-done.6, ...), custom_call_target="tpu_custom_call" | custom-call | flops 805306368 | bytes 1048576 | tf_op jit(solution)/shard_map/pallas_call | solution.py:284
  11.2 0.0 collective-permute-done.3.refs_3_
  11.3 0.3 collective-permute-done.2.refs_2_
  11.5 3.5 %collective-permute-done.1.refs_1_ = s32[2,8,8]{2,1,0:T(8,128)S(1)} collective-permute-done((s32[2,8,8]{2,1,0:T(8,128)S(1)}, s32[2,8,8]{2,1,0:T(8,128)S(1)}, u32[]{:S(2)}, u32[]{:S(2)}) %collective-permute-start.1) | collective-permute-done | bytes 544 | tf_op jit(solution)/shard_map/ppermute | solution.py:278
  15.0 0.9 %shard_map.103 = bf16[8,64,128]{2,1,0:T(8,128)(2,1)} custom-call(s32[1,8,8]{2,1,0:T(8,128)S(1)} %collective-permute-done.refs_0_, s32[2,8,8]{2,1,0:T(8,128)S(1)} %collective-permute-done.1.refs_1_, s32[2,8,8]{2,1,0:T(8,128)S(1)} %collective-permute-done.2.refs_2_, s32[2,8,8]{2,1,0:T(8,128)S(1)} %collective-permute-done.3.refs_3_, ...), custom_call_target="tpu_custom_call" | custom-call | flops 1000000 | bytes 1048576 | tf_op jit(solution)/shard_map/pallas_call | solution.py:295
  15.9 3.4 %all-to-all-start = ((bf16[8,64,128]{2,1,0:T(8,128)(2,1)}), bf16[8,64,128]{2,1,0:T(8,128)(2,1)S(1)}, u32[]{:S(2)}, u32[]{:S(2)}) async-start(bf16[8,64,128]{2,1,0:T(8,128)(2,1)} %shard_map.103), calls=%async_computation | async-start | bytes 262144 | tf_op jit(solution)/shard_map/all_to_all | solution.py:302
  19.3 1.7 %shard_map.102 = (f32[512,256]{1,0:T(8,128)S(1)}, bf16[512,256]{1,0:T(8,128)(2,1)S(1)}) custom-call(bf16[512,256]{1,0:T(8,128)(2,1)S(1)} %get-tuple-element.9.q_ref, bf16[512,128]{1,0:T(8,128)(2,1)S(1)} %get-tuple-element.10.pair_ref.refs_4_, s32[8,8]{1,0:T(8,128)S(1)} %bitcast.9), custom_call_target="tpu_custom_call" | custom-call | flops 2000000000 | bytes 1048576 | tf_op jit(solution)/shard_map/pallas_call | solution.py:304
  20.9 0.0 copy-start
  21.0 0.0 copy-start.8
  21.0 5.6 %all-to-all-done = bf16[8,64,128]{2,1,0:T(8,128)(2,1)S(1)} async-done(((bf16[8,64,128]{2,1,0:T(8,128)(2,1)}), bf16[8,64,128]{2,1,0:T(8,128)(2,1)S(1)}, u32[]{:S(2)}, u32[]{:S(2)}) %all-to-all-start) | async-done | bytes 131104 | tf_op jit(solution)/shard_map/all_to_all | solution.py:302
  26.6 0.6 %shard_map.105.refs_0_ = bf16[256,256]{1,0:T(8,128)(2,1)S(1)} custom-call(s32[8,8]{1,0:T(8,128)S(1)} %bitcast.10, bf16[512,256]{1,0:T(8,128)(2,1)S(1)} %get-tuple-element.9.q_ref, f32[512,256]{1,0:T(8,128)S(1)} %get-tuple-element.11.lse_ref, bf16[512,128]{1,0:T(8,128)(2,1)S(1)} %bitcast.5, bf16[512,256]{1,0:T(8,128)(2,1)S(1)} %get-tuple-element.12.o_ref), custom_call_target="tpu_custom_call" | custom-call | flops 100000000 | bytes 1048576 | tf_op jit(solution)/shard_map/pallas_call | solution.py:321
  27.2 1.6 %collective-permute-start.7 = (bf16[256,256]{1,0:T(8,128)(2,1)S(1)}, bf16[256,256]{1,0:T(8,128)(2,1)S(1)}, u32[]{:S(2)}, u32[]{:S(2)}) collective-permute-start(bf16[256,256]{1,0:T(8,128)(2,1)S(1)} %shard_map.105.refs_0_), channel_id=1, source_target_pairs={{0,2},{1,3},{2,0},{3,1},{4,6},{5,7},{6,4},{7,5},{8,10},{9,11},{10,... | collective-permute-start | bytes 393224 | tf_op jit(solution)/shard_map/ppermute | solution.py:328
  28.7 0.6 %shard_map.104.refs_0_ = bf16[256,256]{1,0:T(8,128)(2,1)S(1)} custom-call(s32[8,8]{1,0:T(8,128)S(1)} %bitcast.11, bf16[512,256]{1,0:T(8,128)(2,1)S(1)} %get-tuple-element.9.q_ref, f32[512,256]{1,0:T(8,128)S(1)} %get-tuple-element.11.lse_ref, bf16[512,128]{1,0:T(8,128)(2,1)S(1)} %bitcast.6, bf16[512,256]{1,0:T(8,128)(2,1)S(1)} %get-tuple-element.12.o_ref), custom_call_target="tpu_custom_call" | custom-call | flops 100000000 | bytes 1048576 | tf_op jit(solution)/shard_map/pallas_call | solution.py:321
  29.3 0.6 %collective-permute-start.4 = (bf16[256,256]{1,0:T(8,128)(2,1)S(1)}, bf16[256,256]{1,0:T(8,128)(2,1)S(1)}, u32[]{:S(2)}, u32[]{:S(2)}) collective-permute-start(bf16[256,256]{1,0:T(8,128)(2,1)S(1)} %shard_map.104.refs_0_), channel_id=1, source_target_pairs={{0,2},{1,3},{2,0},{3,1},{4,6},{5,7},{6,4},{7,5},{8,10},{9,11},{10,... | collective-permute-start | bytes 393224 | tf_op jit(solution)/shard_map/ppermute | solution.py:328
  29.9 0.0 collective-permute-start.8
  29.9 2.3 %collective-permute-done.7.refs_1_ = bf16[256,256]{1,0:T(8,128)(2,1)S(1)} collective-permute-done((bf16[256,256]{1,0:T(8,128)(2,1)S(1)}, bf16[256,256]{1,0:T(8,128)(2,1)S(1)}, u32[]{:S(2)}, u32[]{:S(2)}) %collective-permute-start.7) | collective-permute-done | bytes 131104 | tf_op jit(solution)/shard_map/ppermute | solution.py:328
  32.2 0.0 collective-permute-start.9
  32.2 0.5 %collective-permute-start.5 = (bf16[256,256]{1,0:T(8,128)(2,1)S(1)}, bf16[256,256]{1,0:T(8,128)(2,1)S(1)}, u32[]{:S(2)}, u32[]{:S(2)}) collective-permute-start(bf16[256,256]{1,0:T(8,128)(2,1)S(1)} %shard_map.104.refs_0_), channel_id=1, source_target_pairs={{0,1},{1,0},{2,3},{3,2},{4,5},{5,4},{6,7},{7,6},{8,9},{9,8},{10,11... | collective-permute-start | bytes 393224 | tf_op jit(solution)/shard_map/ppermute | solution.py:335
  32.7 1.6 %collective-permute-done.4.refs_1_ = bf16[256,256]{1,0:T(8,128)(2,1)S(1)} collective-permute-done((bf16[256,256]{1,0:T(8,128)(2,1)S(1)}, bf16[256,256]{1,0:T(8,128)(2,1)S(1)}, u32[]{:S(2)}, u32[]{:S(2)}) %collective-permute-start.4) | collective-permute-done | bytes 131104 | tf_op jit(solution)/shard_map/ppermute | solution.py:328
  34.3 0.0 collective-permute-start.6
  34.4 0.0 collective-permute-done.8.refs_2_
  34.4 0.0 collective-permute-done.9.refs_3_
  34.4 1.2 %shard_map.106.refs_6_ = bf16[512,512]{1,0:T(8,128)(2,1)} custom-call(bf16[256,256]{1,0:T(8,128)(2,1)S(1)} %shard_map.105.refs_0_, bf16[256,256]{1,0:T(8,128)(2,1)S(1)} %collective-permute-done.7.refs_1_, bf16[256,256]{1,0:T(8,128)(2,1)S(1)} %collective-permute-done.8.refs_2_, bf16[256,256]{1,0:T(8,128)(2,1)S(1)} %collective-permute-done.9.refs_3_, ...), custom_call_target="tpu_custom_call" | custom-call | flops 268435456 | bytes 1048576 | tf_op jit(solution)/shard_map/pallas_call | solution.py:339
  35.6 0.0 collective-permute-done.5.refs_2_
  35.6 0.1 collective-permute-done.6.refs_3_
  35.7 1.2 %shard_map.107 = bf16[512,512]{1,0:T(8,128)(2,1)} custom-call(bf16[256,256]{1,0:T(8,128)(2,1)S(1)} %shard_map.104.refs_0_, bf16[256,256]{1,0:T(8,128)(2,1)S(1)} %collective-permute-done.4.refs_1_, bf16[256,256]{1,0:T(8,128)(2,1)S(1)} %collective-permute-done.5.refs_2_, ...), custom_call_target="tpu_custom_call", output_to_operand_aliasing={{}: (6, {})} | custom-call | flops 268435456 | bytes 1048576 | tf_op jit(solution)/shard_map/pallas_call | solution.py:339
  (20 shorter events, 0.0 us)
Async XLA Ops:
  0.0 9.6 %copy-start.5 = (f32[512,128]{1,0:T(8,128)S(1)}, f32[512,128]{1,0:T(8,128)}, u32[]{:S(2)}) copy-start(f32[512,128]{1,0:T(8,128)} %constant.7.clone.sin_ref) | copy-start | bytes 786436
  0.0 9.6 %copy-start.6 = (f32[512,128]{1,0:T(8,128)S(1)}, f32[512,128]{1,0:T(8,128)}, u32[]{:S(2)}) copy-start(f32[512,128]{1,0:T(8,128)} %constant.6.clone.cos_ref) | copy-start | bytes 786436
  0.0 9.6 %copy-start.9 = (f32[8,256]{1,0:T(8,128)S(1)}, f32[8,256]{1,0:T(8,128)}, u32[]{:S(2)}) copy-start(f32[8,256]{1,0:T(8,128)} %constant.8.clone.place_ref) | copy-start | bytes 24580
  0.0 3.1 %copy-start.7 = (s32[1,8,8]{2,1,0:T(8,128)S(1)}, s32[1,8,8]{2,1,0:T(8,128)}, u32[]{:S(2)}) copy-start(s32[1,8,8]{2,1,0:T(8,128)} %param.16) | copy-start | bytes 772
  0.0 9.6 %copy-start.4 = (bf16[2048,64]{0,1:T(8,128)(2,1)S(1)}, bf16[2048,64]{0,1:T(8,128)(2,1)}, u32[]{:S(2)}) copy-start(bf16[2048,64]{0,1:T(8,128)(2,1)} %param.13) | copy-start | bytes 786436
  0.0 9.6 %copy-start.3 = (bf16[2048,64]{0,1:T(8,128)(2,1)S(1)}, bf16[2048,64]{0,1:T(8,128)(2,1)}, u32[]{:S(2)}) copy-start(bf16[2048,64]{0,1:T(8,128)(2,1)} %param.12) | copy-start | bytes 786436
  0.0 9.6 %copy-start.2 = (bf16[2048,256]{1,0:T(8,128)(2,1)S(1)}, bf16[2048,256]{1,0:T(8,128)(2,1)}, u32[]{:S(2)}) copy-start(bf16[2048,256]{1,0:T(8,128)(2,1)} %wq_ref.1) | copy-start | bytes 3145732
  0.0 9.6 %copy-start.1 = (bf16[512,2048]{1,0:T(8,128)(2,1)S(1)}, bf16[512,2048]{1,0:T(8,128)(2,1)}, u32[]{:S(2)}) copy-start(bf16[512,2048]{1,0:T(8,128)(2,1)} %x_ref.1) | copy-start | bytes 6291460
  0.0 4.9 %collective-permute-start = (s32[1,8,8]{2,1,0:T(8,128)}, s32[1,8,8]{2,1,0:T(8,128)S(1)}, u32[]{:S(2)}, u32[]{:S(2)}) collective-permute-start(s32[1,8,8]{2,1,0:T(8,128)} %param.16), channel_id=1, source_target_pairs={{0,4},{4,0},{8,12},{12,8},{16,20},{20,16},{24,28},{28,24},{1,5},{5... | collective-permute-start | bytes 776 | tf_op jit(solution)/shard_map/ppermute | solution.py:274
  4.9 6.3 %collective-permute-start.3 = (s32[2,8,8]{2,1,0:T(8,128)S(1)}, s32[2,8,8]{2,1,0:T(8,128)S(1)}, u32[]{:S(2)}, u32[]{:S(2)}) collective-permute-start(s32[2,8,8]{2,1,0:T(8,128)S(1)} %constant_dynamic-update-slice_fusion), channel_id=1, source_target_pairs={{0,8},{4,12},{8,0},{12,4},{16,24},{20,28},{24,16},{28,20},{1,9},{5... | collective-permute-start | bytes 1544 | tf_op jit(solution)/shard_map/ppermute | solution.py:278
  7.0 4.5 %collective-permute-start.2 = (s32[2,8,8]{2,1,0:T(8,128)S(1)}, s32[2,8,8]{2,1,0:T(8,128)S(1)}, u32[]{:S(2)}, u32[]{:S(2)}) collective-permute-start(s32[2,8,8]{2,1,0:T(8,128)S(1)} %constant_dynamic-update-slice_fusion), channel_id=1, source_target_pairs={{0,16},{4,20},{8,24},{12,28},{16,0},{20,4},{24,8},{28,12},{1,17},{... | collective-permute-start | bytes 1544 | tf_op jit(solution)/shard_map/ppermute | solution.py:278
  9.6 5.4 %collective-permute-start.1 = (s32[2,8,8]{2,1,0:T(8,128)S(1)}, s32[2,8,8]{2,1,0:T(8,128)S(1)}, u32[]{:S(2)}, u32[]{:S(2)}) collective-permute-start(s32[2,8,8]{2,1,0:T(8,128)S(1)} %constant_dynamic-update-slice_fusion), channel_id=1, source_target_pairs={{0,24},{4,28},{8,16},{12,20},{16,8},{20,12},{24,0},{28,4},{1,25},{... | collective-permute-start | bytes 1544 | tf_op jit(solution)/shard_map/ppermute | solution.py:278
  15.9 10.7 %all-to-all-start = ((bf16[8,64,128]{2,1,0:T(8,128)(2,1)}), bf16[8,64,128]{2,1,0:T(8,128)(2,1)S(1)}, u32[]{:S(2)}, u32[]{:S(2)}) async-start(bf16[8,64,128]{2,1,0:T(8,128)(2,1)} %shard_map.103), calls=%async_computation | async-start | bytes 262144 | tf_op jit(solution)/shard_map/all_to_all | solution.py:302
  20.9 13.4 %copy-start = (bf16[1024,512]{1,0:T(8,128)(2,1)S(1)}, bf16[1024,512]{1,0:T(8,128)(2,1)}, u32[]{:S(2)}) copy-start(bf16[1024,512]{1,0:T(8,128)(2,1)} %refs_5_.3) | copy-start | bytes 3145732
  21.0 13.4 %copy-start.8 = (f32[1024]{0:T(1024)S(1)}, f32[1024]{0:T(1024)}, u32[]{:S(2)}) copy-start(f32[1024]{0:T(1024)} %param.15) | copy-start | bytes 12292
  27.2 5.0 %collective-permute-start.7 = (bf16[256,256]{1,0:T(8,128)(2,1)S(1)}, bf16[256,256]{1,0:T(8,128)(2,1)S(1)}, u32[]{:S(2)}, u32[]{:S(2)}) collective-permute-start(bf16[256,256]{1,0:T(8,128)(2,1)S(1)} %shard_map.105.refs_0_), channel_id=1, source_target_pairs={{0,2},{1,3},{2,0},{3,1},{4,6},{5,7},{6,4},{7,5},{8,10},{9,11},{10,... | collective-permute-start | bytes 393224 | tf_op jit(solution)/shard_map/ppermute | solution.py:328
  29.3 5.0 %collective-permute-start.4 = (bf16[256,256]{1,0:T(8,128)(2,1)S(1)}, bf16[256,256]{1,0:T(8,128)(2,1)S(1)}, u32[]{:S(2)}, u32[]{:S(2)}) collective-permute-start(bf16[256,256]{1,0:T(8,128)(2,1)S(1)} %shard_map.104.refs_0_), channel_id=1, source_target_pairs={{0,2},{1,3},{2,0},{3,1},{4,6},{5,7},{6,4},{7,5},{8,10},{9,11},{10,... | collective-permute-start | bytes 393224 | tf_op jit(solution)/shard_map/ppermute | solution.py:328
  29.9 4.4 %collective-permute-start.8 = (bf16[256,256]{1,0:T(8,128)(2,1)S(1)}, bf16[256,256]{1,0:T(8,128)(2,1)S(1)}, u32[]{:S(2)}, u32[]{:S(2)}) collective-permute-start(bf16[256,256]{1,0:T(8,128)(2,1)S(1)} %shard_map.105.refs_0_), channel_id=1, source_target_pairs={{0,1},{1,0},{2,3},{3,2},{4,5},{5,4},{6,7},{7,6},{8,9},{9,8},{10,11... | collective-permute-start | bytes 393224 | tf_op jit(solution)/shard_map/ppermute | solution.py:335
  32.2 2.2 %collective-permute-start.9 = (bf16[256,256]{1,0:T(8,128)(2,1)S(1)}, bf16[256,256]{1,0:T(8,128)(2,1)S(1)}, u32[]{:S(2)}, u32[]{:S(2)}) collective-permute-start(bf16[256,256]{1,0:T(8,128)(2,1)S(1)} %collective-permute-done.7.refs_1_), channel_id=1, source_target_pairs={{0,1},{1,0},{2,3},{3,2},{4,5},{5,4},{6,7},{7,6},{8,9},{9,8},{10,11... | collective-permute-start | bytes 393224 | tf_op jit(solution)/shard_map/ppermute | solution.py:335
  32.2 3.4 %collective-permute-start.5 = (bf16[256,256]{1,0:T(8,128)(2,1)S(1)}, bf16[256,256]{1,0:T(8,128)(2,1)S(1)}, u32[]{:S(2)}, u32[]{:S(2)}) collective-permute-start(bf16[256,256]{1,0:T(8,128)(2,1)S(1)} %shard_map.104.refs_0_), channel_id=1, source_target_pairs={{0,1},{1,0},{2,3},{3,2},{4,5},{5,4},{6,7},{7,6},{8,9},{9,8},{10,11... | collective-permute-start | bytes 393224 | tf_op jit(solution)/shard_map/ppermute | solution.py:335
  34.3 1.3 %collective-permute-start.6 = (bf16[256,256]{1,0:T(8,128)(2,1)S(1)}, bf16[256,256]{1,0:T(8,128)(2,1)S(1)}, u32[]{:S(2)}, u32[]{:S(2)}) collective-permute-start(bf16[256,256]{1,0:T(8,128)(2,1)S(1)} %collective-permute-done.4.refs_1_), channel_id=1, source_target_pairs={{0,1},{1,0},{2,3},{3,2},{4,5},{5,4},{6,7},{7,6},{8,9},{9,8},{10,11... | collective-permute-start | bytes 393224 | tf_op jit(solution)/shard_map/ppermute | solution.py:335

commit v2 on v1

--- a/solution.py
+++ b/solution.py
@@ -25,16 +25,13 @@
 def rope_tables(rows, places):
     half = HD // 2
     frequency = ROPE_BASE ** (-np.arange(half, dtype=np.float64) / half)
-    reps = LANES // half
-
-    def both(positions):
+
+    def packed(positions):
         angles = positions[:, None].astype(np.float64) * frequency[None, :]
-        wide = np.tile(angles, (1, reps))
-        return np.cos(wide).astype(np.float32), np.sin(wide).astype(np.float32)
-
-    row_cos, row_sin = both(np.arange(rows))
-    place_cos, place_sin = both(np.arange(places) * rows)
-    return row_cos, row_sin, np.concatenate([place_cos, place_sin], axis=1)
+        pair = np.concatenate([np.cos(angles), np.sin(angles)], axis=1)
+        return np.tile(pair, (1, LANES // HD)).astype(np.float32)
+
+    return packed(np.arange(rows)), packed(np.arange(places) * rows)
 
 
 def vmem():
@@ -57,13 +54,20 @@
     return lax.broadcasted_iota(jnp.int32, shape, len(shape) - 1)
 
 
-def cos_sin(cos_ref, sin_ref, place_ref, sign_ref):
+def cos_sin(row_ref, place_ref, sign_ref):
+    half = HD // 2
+
+    def unpack(packed):
+        low = lane_index(packed.shape) % HD < half
+        cosine = jnp.where(low, packed, pltpu.roll(packed, half, 1))
+        sine = jnp.where(low, pltpu.roll(packed, LANES - half, 1), packed)
+        return cosine, sine
+
+    rc, rs = unpack(row_ref[...])
     place = place_ref[pl.ds(lax.axis_index("kv"), 1), :]
-    pc, ps = place[:, :LANES], place[:, LANES:]
-    rc, rs = cos_ref[...], sin_ref[...]
-    cosine = rc * pc - rs * ps
-    sine = rs * pc + rc * ps
-    return cosine, sine * sign_ref[0:1, :]
+    pc, ps = unpack(jnp.broadcast_to(place, (8, LANES)))
+    pc, ps = pc[0:1], ps[0:1]
+    return rc * pc - rs * ps, (rs * pc + rc * ps) * sign_ref[0:1, :]
 
 
 def turn(values, cosine, sine):
@@ -79,42 +83,54 @@
     out_ref[...] = jnp.where(first, -1.0, 1.0)
 
 
-def qkv_kernel(
-    x_ref, wk_ref, wv_ref, wq_ref, cos_ref, sin_ref, place_ref, sign_ref, pair_ref, q_ref, wkv_ref
-):
+def kv_kernel(x_ref, wk_ref, wv_ref, row_ref, place_ref, sign_ref, pair_ref, wkv_ref):
     wkv_ref[:HD, :] = wk_ref[...]
     wkv_ref[HD:, :] = wv_ref[...]
     both = lax.dot_general(
         x_ref[...], wkv_ref[...], (((1,), (1,)), ((), ())), preferred_element_type=F32
     )
-    cosine, sine = cos_sin(cos_ref, sin_ref, place_ref, sign_ref)
+    cosine, sine = cos_sin(row_ref, place_ref, sign_ref)
     turned = turn(both, cosine, sine)
     pair_ref[...] = jnp.where(lane_index(both.shape) < HD, turned, both).astype(BF16)
+
+
+def query_kernel(x_ref, wq_ref, row_ref, place_ref, sign_ref, q_ref):
     q = jnp.dot(x_ref[...], wq_ref[...], preferred_element_type=F32)
+    cosine, sine = cos_sin(row_ref, place_ref, sign_ref)
     for j in range(q_ref.shape[1] // LANES):
         lanes = slice(j * LANES, (j + 1) * LANES)
         q_ref[:, lanes] = (turn(q[:, lanes], cosine, sine) * HD**-0.5).astype(BF16)
 
 
-def pick_kernel(masks, *refs):
-    *table_refs, pair_ref, out_ref = refs
+def wanted(table, owner, blocks):
+    local = table - owner * blocks
+    mine = (local >= 0) & (local < blocks)
+    index = jnp.max(jnp.where(mine, local, 0))
+    return pl.ds(pl.multiple_of(index * BLK, BLK), BLK)
+
+
+def give_kernel(*refs):
+    count = (len(refs) - 2) // 2
+    table_refs, (pair_ref, beside_ref), out_refs = refs[:count], refs[count : count + 2], refs[count + 2 :]
     blocks = pair_ref.shape[0] // BLK
     me = lax.axis_index("kv")
-    first = me * blocks
-
-    def one(peer, table):
-        local = table - first
-        mine = (local >= 0) & (local < blocks)
-        index = jnp.max(jnp.where(mine, local, 0))
-        out_ref[peer] = pair_ref[pl.ds(pl.multiple_of(index * BLK, BLK), BLK), :]
-
-    if masks:
-        out_ref[me] = pair_ref[:BLK, :]
-        for ref, group in zip(table_refs, masks, strict=True):
-            for i, mask in enumerate(group):
-                one(me ^ mask, ref[i])
-    else:
-        pl.loop(0, out_ref.shape[0])(lambda peer: one(peer, table_refs[0][peer]))
+    odd = me & 1
+    for table_ref, out_ref in zip(table_refs, out_refs, strict=True):
+        table = table_ref[0]
+        for owner, ref in ((me, pair_ref), (me ^ 1, beside_ref)):
+            place = odd if ref is pair_ref else 1 - odd
+            at = pl.ds(pl.multiple_of(place * BLK, BLK), BLK)
+            out_ref[at, :] = ref[wanted(table, owner, blocks), :]
+
+
+def pick_kernel(table_ref, pair_ref, out_ref):
+    blocks = pair_ref.shape[0] // BLK
+    me = lax.axis_index("kv")
+
+    def one(peer):
+        out_ref[peer] = pair_ref[wanted(table_ref[peer], me, blocks), :]
+
+    pl.loop(0, out_ref.shape[0])(one)
 
 
 def heads_of(q, count):
@@ -187,12 +203,13 @@
             o_ref[at:span, lanes] = (total / sums).astype(BF16)
 
 
-def remote_kernel(start, ch_ref, q_ref, lse_ref, arr_ref, o_ref, out_ref, seen_ref):
+def remote_kernel(start, masks, ch_ref, q_ref, lse_ref, o_ref, *refs):
+    *key_refs, out_ref, seen_ref = refs
     rows, width = out_ref.shape
     heads = width // HD
     blocks = q_ref.shape[0] // BLK
-    peers = arr_ref.shape[0] // BLK
-    group = 8 if peers % 8 == 0 else peers
+    peers = sum(ref.shape[0] for ref in key_refs) // BLK
+    group = peers if masks else 8
     span = group * BLK
     me = lax.axis_index("kv")
     names = ch_ref[...]
@@ -223,18 +240,32 @@
 
     def one_group(g):
         base = g * group
-        key_peer = lane_index((blocks, span)) // BLK + base
+        key_peer = lane_index((blocks, span)) // BLK
+        if masks:
+            part = key_peer // 2
+            column = jnp.full(part.shape, me & -2, jnp.int32)
+            for i, mask in enumerate(masks):
+                column = jnp.where(part == i, (me ^ mask) & -2, column)
+            key_peer = column + key_peer % 2
+        else:
+            key_peer = key_peer + base
         named = away[:, 0:1] == key_peer
         for s in range(1, names.shape[1]):
             named = named | (away[:, s : s + 1] == key_peer)
         bias = jnp.where(named, 0.0, MASKED)
+        inside = (away >= base) & (away < base + group)
+        place = lax.broadcasted_iota(jnp.int32, away.shape, 0)
+        flags = jnp.max(jnp.where(inside, 1 << place, 0), axis=1, keepdims=True)
+        used = jnp.sum(flags)
         for b in range(rows // BLK):
             row = bias[start // BLK + b : start // BLK + b + 1]
-            used = jnp.max(row) > -1.0
-
-            @pl.when(used)
+
+            @pl.when((used >> (start // BLK + b)) & 1 == 1)
             def _():
-                keys = arr_ref[pl.ds(pl.multiple_of(base * BLK, span), span), :]
+                if masks:
+                    keys = jnp.concatenate([ref[...] for ref in key_refs], axis=0)
+                else:
+                    keys = key_refs[0][pl.ds(pl.multiple_of(base * BLK, span), span), :]
                 block(b, jnp.broadcast_to(row, (BLK, span)), keys)
 
     if peers == group:
@@ -267,39 +298,46 @@
     rows, depth = tokens.shape
     width = w_query.shape[1]
     names = chosen[0]
-    row_cos, row_sin, place = (jnp.asarray(t) for t in tables)
+    row_table, place_table = (jnp.asarray(t) for t in tables)
     sign = call(sign_kernel, jax.ShapeDtypeStruct((8, LANES), F32), 0, SIGN_FLOPS, mib=1)()
+    turns = (row_table, place_table, sign)
+    pair_shape = jax.ShapeDtypeStruct((rows, LANES), BF16)
+    pairs = call(
+        kv_kernel,
+        pair_shape,
+        6,
+        2 * rows * depth * LANES,
+        [pltpu.VMEM((LANES, depth), BF16)],
+        mib=8,
+    )(tokens, w_key.T, w_value.T, *turns)
+    q = call(
+        query_kernel, jax.ShapeDtypeStruct((rows, width), BF16), 5, 2 * rows * depth * width, mib=8
+    )(tokens, w_query, *turns)
     if spread(peers):
         swap = {m: [(i, i ^ m) for i in range(peers)] for m in range(1, peers)}
-        beside = lax.ppermute(chosen, "kv", swap[1])
-        both = jnp.concatenate([chosen, beside], axis=0)
-        asked, masks = [beside], [(1,)]
-        for m in range(peers - 2, 0, -2):
-            asked.append(lax.ppermute(both, "kv", swap[m]))
-            masks.append((m, m ^ 1))
+        far = list(range(peers - 2, 0, -2))
+        asked = [chosen]
+        for m in far:
+            asked.append(lax.ppermute(chosen, "kv", swap[m]))
+        beside = lax.ppermute(pairs, "kv", swap[1])
+        given = call(
+            give_kernel,
+            tuple(jax.ShapeDtypeStruct((PAIR, LANES), BF16) for _ in asked),
+            len(asked) + 2,
+            10**6,
+            mib=4,
+        )(*asked, pairs, beside)
+        arrived = [given[0]]
+        for m, blocks in zip(far, given[1:], strict=True):
+            arrived.append(lax.ppermute(blocks, "kv", swap[m]))
+        masks = (0, *far)
     else:
         table = jnp.broadcast_to(names[None], (peers, *names.shape))
-        asked = [lax.all_to_all(table, "kv", 0, 0, tiled=True)]
-        masks = []
-    pairs, q = call(
-        qkv_kernel,
-        (
-            jax.ShapeDtypeStruct((rows, LANES), BF16),
-            jax.ShapeDtypeStruct((rows, width), BF16),
-        ),
-        8,
-        2 * rows * depth * (LANES + width),
-        [pltpu.VMEM((LANES, depth), BF16)],
-        mib=16,
-    )(tokens, w_key.T, w_value.T, w_query, row_cos, row_sin, place, sign)
-    outgoing = call(
-        functools.partial(pick_kernel, masks),
-        jax.ShapeDtypeStruct((peers, BLK, LANES), BF16),
-        len(asked) + 1,
-        10**6,
-        mib=4,
-    )(*asked, pairs)
-    arrived = lax.all_to_all(outgoing, "kv", 0, 0, tiled=True).reshape(peers * BLK, LANES)
+        outgoing = call(
+            pick_kernel, jax.ShapeDtypeStruct((peers, BLK, LANES), BF16), 2, 10**6, mib=8
+        )(lax.all_to_all(table, "kv", 0, 0, tiled=True), pairs)
+        arrived = [lax.all_to_all(outgoing, "kv", 0, 0, tiled=True).reshape(peers * BLK, LANES)]
+        masks = ()
     step = rows // CHUNKS
     lse, attended = call(
         local_kernel,
@@ -319,12 +357,12 @@
     sent = []
     for c in reversed(range(CHUNKS)):
         mixed = call(
-            functools.partial(remote_kernel, c * step),
+            functools.partial(remote_kernel, c * step, masks),
             jax.ShapeDtypeStruct((step, width), BF16),
-            5,
+            4 + len(arrived),
             10**8,
-            [pltpu.VMEM((step, width) if peers > 8 else (8, LANES), F32)],
-        )(names, q, lse, arrived, attended)
+            [pltpu.VMEM((8, LANES) if masks else (step, width), F32)],
+        )(names, q, lse, attended, *arrived)
         sent.append((c, [mixed, lax.ppermute(mixed, "tp", swaps[flips[0]])]))
     result = None
     for c, held in sent:

time: 37.1 us -> 30.5 us (0.82)
  waiting for transfers between devices: 15.2 us -> 7.7 us
  local copies, waits for them, and re-layouts: 0.05 us -> 1.74 us
  Pallas kernels: 7.66 us -> 6.42 us
  starting transfers between devices: 13.8 us -> 14.4 us
    all_to_all x1 -> x0, waiting for transfers between devices: 5.59 us -> none  [per_device(): lax.all_to_all(outgoing, 'kv', 0, 0, tiled=True).reshape(peers * BLK, LANES)]
    ppermute x4 -> x7, starting transfers between devices: 7.74 us -> 11.7 us  [the longest x3 4.45 us: per_device(): arrived.append(lax.ppermute(blocks, 'kv', swap[m]))]
    all_to_all x1 -> x0, starting transfers between devices: 3.37 us -> none  [per_device(): lax.all_to_all(outgoing, 'kv', 0, 0, tiled=True).reshape(peers * BLK, LANES)]
    ppermute x4 -> x7, waiting for transfers between devices: 5.57 us -> 3.64 us  [the longest x3 2.88 us: per_device(): asked.append(lax.ppermute(chosen, 'kv', swap[m]))]
    unnamed x21 -> x18, local copies, waits for them, and re-layouts: 0.05 us -> 1.74 us
    pallas_call x4 -> x5, Pallas kernels: 3.63 us -> 2.4 us  [the longest x1 0.93 us: per_device(): call(query_kernel, jax.ShapeDtypeStruct((rows, width), BF16), 5, 2 * rows...]
  transfers between devices with their start and end apart: 11 -> 13, of which waited for: 7 -> 5; matrix products, arithmetic and copies ran while one was open for 0% -> 0% of each run, Pallas kernels for 14% -> 13%
where the time goes in v2:
time: 30.5 us; the launch traced here: 30.3 us
  starting transfers between devices  14.4 us (47%)
  waiting for transfers between devices  7.7 us (25%)
  Pallas kernels  6.42 us (21%)
  local copies, waits for them, and re-layouts  1.74 us (6%)
    ppermute x3, starting transfers between devices, per_device(): arrived.append(lax.ppermute(blocks, 'kv', swap[m]))  4.45 us
    ppermute x3, starting transfers between devices, per_device(): asked.append(lax.ppermute(chosen, 'kv', swap[m]))  4.17 us
    ppermute x2, waiting for transfers between devices, per_device(): sent.append((c, [mixed, lax.ppermute(mixed, 'tp', swaps[flips[0]])]))  3.92 us
    ppermute x1, starting transfers between devices, per_device(): beside = lax.ppermute(pairs, 'kv', swap[1])  3.06 us
    ppermute x3, waiting for transfers between devices, per_device(): asked.append(lax.ppermute(chosen, 'kv', swap[m]))  2.88 us
    pallas_call x2, Pallas kernels, per_device(): pl.pallas_call(functools.partial(out_kernel, columns, masks), out_shape=j...  2.35 us
    ppermute x2, starting transfers between devices, per_device(): sent.append((c, [mixed, lax.ppermute(mixed, 'tp', swaps[flips[0]])]))  2.16 us
    unnamed x18, local copies, waits for them, and re-layouts  1.74 us
  transfers between devices with their start and end apart: 13, of which 5 were waited for; matrix products, arithmetic and copies ran while one was open for 0% of the time, Pallas kernels for 13%

profile of v2, /device:TPU:0, one launch (start us, length us, event | category | flops | bytes accessed | tf_op | source)
XLA Modules:
  0.0 30.3 jit_solution(6465275854985793262)
XLA Ops:
  0.0 0.0 copy-start.6
  0.0 0.0 copy-start.3
  0.1 0.9 %copy-done.2 = f32[512,128]{1,0:T(8,128)S(1)} copy-done((f32[512,128]{1,0:T(8,128)S(1)}, f32[512,128]{1,0:T(8,128)}, u32[]{:S(2)}) %copy-start.2) | copy-done | bytes 262168
  1.0 0.8 %copy-done = bf16[512,2048]{1,0:T(8,128)(2,1)S(1)} copy-done((bf16[512,2048]{1,0:T(8,128)(2,1)S(1)}, bf16[512,2048]{1,0:T(8,128)(2,1)}, u32[]{:S(2)}) %copy-start) | copy-done | bytes 2097176
  1.7 0.0 copy-done.4
  1.8 0.8 %shard_map.93.pair_ref.refs_4_ = bf16[512,128]{1,0:T(8,128)(2,1)S(1)} custom-call(bf16[512,2048]{1,0:T(8,128)(2,1)S(1)} %copy-done, bf16[64,2048]{1,0:T(8,128)(2,1)S(1)} %bitcast.4, bf16[64,2048]{1,0:T(8,128)(2,1)S(1)} %bitcast.5, f32[512,128]{1,0:T(8,128)S(1)} %copy-done.2, f32[8,128]{1,0:T(8,128)S(1)} %copy-done.8, f32[8,128]{1,0:T(8,128)S(1)} %shard_map.91.sign_ref), custom_call_target="tpu_custom_call" | custom-call | flops 268435456 | bytes 1048576 | tf_op jit(solution)/shard_map/pallas_call | solution.py:305
  2.6 3.1 %collective-permute-start.3 = (bf16[512,128]{1,0:T(8,128)(2,1)S(1)}, bf16[512,128]{1,0:T(8,128)(2,1)S(1)}, u32[]{:S(2)}, u32[]{:S(2)}) collective-permute-start(bf16[512,128]{1,0:T(8,128)(2,1)S(1)} %shard_map.93.pair_ref.refs_4_), channel_id=1, source_target_pairs={{0,4},{4,0},{8,12},{12,8},{16,20},{20,16},{24,28},{28,24},{1,5},{5... | collective-permute-start | bytes 393224 | tf_op jit(solution)/shard_map/ppermute | solution.py:322
  5.6 2.6 %collective-permute-start.1 = (s32[1,8,8]{2,1,0:T(8,128)S(1)}, s32[1,8,8]{2,1,0:T(8,128)S(1)}, u32[]{:S(2)}, u32[]{:S(2)}) collective-permute-start(s32[1,8,8]{2,1,0:T(8,128)S(1)} %copy-done.6), channel_id=1, source_target_pairs={{0,16},{4,20},{8,24},{12,28},{16,0},{20,4},{24,8},{28,12},{1,17},{... | collective-permute-start | bytes 776 | tf_op jit(solution)/shard_map/ppermute | solution.py:321
  8.2 1.3 %collective-permute-start = (s32[1,8,8]{2,1,0:T(8,128)S(1)}, s32[1,8,8]{2,1,0:T(8,128)S(1)}, u32[]{:S(2)}, u32[]{:S(2)}) collective-permute-start(s32[1,8,8]{2,1,0:T(8,128)S(1)} %copy-done.6), channel_id=1, source_target_pairs={{0,24},{4,28},{8,16},{12,20},{16,8},{20,12},{24,0},{28,4},{1,25},{... | collective-permute-start | bytes 776 | tf_op jit(solution)/shard_map/ppermute | solution.py:321
  9.6 0.2 collective-permute-start.2
  9.8 0.9 %shard_map.92.q_ref = bf16[512,256]{1,0:T(8,128)(2,1)S(1)} custom-call(bf16[512,2048]{1,0:T(8,128)(2,1)S(1)} %copy-done, bf16[2048,256]{1,0:T(8,128)(2,1)S(1)} %copy-done.3, f32[512,128]{1,0:T(8,128)S(1)} %copy-done.2, f32[8,128]{1,0:T(8,128)S(1)} %copy-done.8, f32[8,128]{1,0:T(8,128)S(1)} %shard_map.91.sign_ref), custom_call_target="tpu_custom_call" | custom-call | flops 536870912 | bytes 1048576 | tf_op jit(solution)/shard_map/pallas_call | solution.py:313
  10.7 0.0 collective-permute-done.1.refs_2_
  10.7 2.9 %collective-permute-done.refs_1_ = s32[1,8,8]{2,1,0:T(8,128)S(1)} collective-permute-done((s32[1,8,8]{2,1,0:T(8,128)S(1)}, s32[1,8,8]{2,1,0:T(8,128)S(1)}, u32[]{:S(2)}, u32[]{:S(2)}) %collective-permute-start) | collective-permute-done | bytes 288 | tf_op jit(solution)/shard_map/ppermute | solution.py:321
  13.6 0.0 collective-permute-done.3.refs_5_
  13.6 0.2 shard_map.95
  13.8 2.1 %collective-permute-start.4 = (bf16[128,128]{1,0:T(8,128)(2,1)S(1)}, bf16[128,128]{1,0:T(8,128)(2,1)S(1)}, u32[]{:S(2)}, u32[]{:S(2)}) collective-permute-start(bf16[128,128]{1,0:T(8,128)(2,1)S(1)} %get-tuple-element.14), channel_id=1, source_target_pairs={{0,24},{4,28},{8,16},{12,20},{16,8},{20,12},{24,0},{28,4},{1,25},{... | collective-permute-start | bytes 98312 | tf_op jit(solution)/shard_map/ppermute | solution.py:332
  15.9 0.0 collective-permute-start.5
  15.9 2.4 %collective-permute-start.6 = (bf16[128,128]{1,0:T(8,128)(2,1)S(1)}, bf16[128,128]{1,0:T(8,128)(2,1)S(1)}, u32[]{:S(2)}, u32[]{:S(2)}) collective-permute-start(bf16[128,128]{1,0:T(8,128)(2,1)S(1)} %get-tuple-element.16), channel_id=1, source_target_pairs={{0,8},{4,12},{8,0},{12,4},{16,24},{20,28},{24,16},{28,20},{1,9},{5... | collective-permute-start | bytes 98312 | tf_op jit(solution)/shard_map/ppermute | solution.py:332
  18.3 1.7 %shard_map.94 = (f32[512,256]{1,0:T(8,128)S(1)}, bf16[512,256]{1,0:T(8,128)(2,1)S(1)}) custom-call(bf16[512,256]{1,0:T(8,128)(2,1)S(1)} %shard_map.92.q_ref, bf16[512,128]{1,0:T(8,128)(2,1)S(1)} %shard_map.93.pair_ref.refs_4_, s32[8,8]{1,0:T(8,128)S(1)} %bitcast.6), custom_call_target="tpu_custom_call" | custom-call | flops 2000000000 | bytes 1048576 | tf_op jit(solution)/shard_map/pallas_call | solution.py:342
  20.0 0.0 copy-start.1
  20.0 0.0 copy-start.7
  20.0 0.7 %collective-permute-done.5.refs_2_ = bf16[128,128]{1,0:T(8,128)(2,1)S(1)} collective-permute-done((bf16[128,128]{1,0:T(8,128)(2,1)S(1)}, bf16[128,128]{1,0:T(8,128)(2,1)S(1)}, u32[]{:S(2)}, u32[]{:S(2)}) %collective-permute-start.5) | collective-permute-done | bytes 32800 | tf_op jit(solution)/shard_map/ppermute | solution.py:332
  20.7 0.2 shard_map.97.refs_0_
  21.0 1.6 %collective-permute-start.10 = (bf16[256,256]{1,0:T(8,128)(2,1)S(1)}, bf16[256,256]{1,0:T(8,128)(2,1)S(1)}, u32[]{:S(2)}, u32[]{:S(2)}) collective-permute-start(bf16[256,256]{1,0:T(8,128)(2,1)S(1)} %shard_map.97.refs_0_), channel_id=1, source_target_pairs={{0,2},{1,3},{2,0},{3,1},{4,6},{5,7},{6,4},{7,5},{8,10},{9,11},{10,... | collective-permute-start | bytes 393224 | tf_op jit(solution)/shard_map/ppermute | solution.py:366
  22.5 0.2 shard_map.96.refs_0_
  22.8 0.6 %collective-permute-start.7 = (bf16[256,256]{1,0:T(8,128)(2,1)S(1)}, bf16[256,256]{1,0:T(8,128)(2,1)S(1)}, u32[]{:S(2)}, u32[]{:S(2)}) collective-permute-start(bf16[256,256]{1,0:T(8,128)(2,1)S(1)} %shard_map.96.refs_0_), channel_id=1, source_target_pairs={{0,2},{1,3},{2,0},{3,1},{4,6},{5,7},{6,4},{7,5},{8,10},{9,11},{10,... | collective-permute-start | bytes 393224 | tf_op jit(solution)/shard_map/ppermute | solution.py:366
  23.4 2.6 %collective-permute-done.10.refs_1_ = bf16[256,256]{1,0:T(8,128)(2,1)S(1)} collective-permute-done((bf16[256,256]{1,0:T(8,128)(2,1)S(1)}, bf16[256,256]{1,0:T(8,128)(2,1)S(1)}, u32[]{:S(2)}, u32[]{:S(2)}) %collective-permute-start.10) | collective-permute-done | bytes 131104 | tf_op jit(solution)/shard_map/ppermute | solution.py:366
  26.0 0.5 %collective-permute-start.8 = (bf16[256,256]{1,0:T(8,128)(2,1)S(1)}, bf16[256,256]{1,0:T(8,128)(2,1)S(1)}, u32[]{:S(2)}, u32[]{:S(2)}) collective-permute-start(bf16[256,256]{1,0:T(8,128)(2,1)S(1)} %shard_map.96.refs_0_), channel_id=1, source_target_pairs={{0,1},{1,0},{2,3},{3,2},{4,5},{5,4},{6,7},{7,6},{8,9},{9,8},{10,11... | collective-permute-start | bytes 393224 | tf_op jit(solution)/shard_map/ppermute | solution.py:373
  26.5 1.3 %collective-permute-done.7.refs_1_ = bf16[256,256]{1,0:T(8,128)(2,1)S(1)} collective-permute-done((bf16[256,256]{1,0:T(8,128)(2,1)S(1)}, bf16[256,256]{1,0:T(8,128)(2,1)S(1)}, u32[]{:S(2)}, u32[]{:S(2)}) %collective-permute-start.7) | collective-permute-done | bytes 131104 | tf_op jit(solution)/shard_map/ppermute | solution.py:366
  27.9 1.2 %shard_map.98.refs_6_ = bf16[512,512]{1,0:T(8,128)(2,1)} custom-call(bf16[256,256]{1,0:T(8,128)(2,1)S(1)} %shard_map.97.refs_0_, bf16[256,256]{1,0:T(8,128)(2,1)S(1)} %collective-permute-done.10.refs_1_, bf16[256,256]{1,0:T(8,128)(2,1)S(1)} %collective-permute-done.11.refs_2_, bf16[256,256]{1,0:T(8,128)(2,1)S(1)} %collective-permute-done.12.refs_3_, ...), custom_call_target="tpu_custom_call" | custom-call | flops 268435456 | bytes 1048576 | tf_op jit(solution)/shard_map/pallas_call | solution.py:377
  29.0 0.1 collective-permute-done.9.refs_3_
  29.2 1.2 %shard_map.99 = bf16[512,512]{1,0:T(8,128)(2,1)} custom-call(bf16[256,256]{1,0:T(8,128)(2,1)S(1)} %shard_map.96.refs_0_, bf16[256,256]{1,0:T(8,128)(2,1)S(1)} %collective-permute-done.7.refs_1_, bf16[256,256]{1,0:T(8,128)(2,1)S(1)} %collective-permute-done.8.refs_2_, ...), custom_call_target="tpu_custom_call", output_to_operand_aliasing={{}: (6, {})} | custom-call | flops 268435456 | bytes 1048576 | tf_op jit(solution)/shard_map/pallas_call | solution.py:377
  (21 shorter events, 0.0 us)
Async XLA Ops:
  0.0 0.9 %copy-start.2 = (f32[512,128]{1,0:T(8,128)S(1)}, f32[512,128]{1,0:T(8,128)}, u32[]{:S(2)}) copy-start(f32[512,128]{1,0:T(8,128)} %constant.4.clone.row_ref) | copy-start | bytes 786436
  0.0 1.0 %copy-start.8 = (f32[8,128]{1,0:T(8,128)S(1)}, f32[8,128]{1,0:T(8,128)}, u32[]{:S(2)}) copy-start(f32[8,128]{1,0:T(8,128)} %constant.5.clone.place_ref) | copy-start | bytes 12292
  0.0 1.7 %copy-start = (bf16[512,2048]{1,0:T(8,128)(2,1)S(1)}, bf16[512,2048]{1,0:T(8,128)(2,1)}, u32[]{:S(2)}) copy-start(bf16[512,2048]{1,0:T(8,128)(2,1)} %x_ref.3) | copy-start | bytes 6291460
  0.0 1.7 %copy-start.5 = (bf16[2048,64]{0,1:T(8,128)(2,1)S(1)}, bf16[2048,64]{0,1:T(8,128)(2,1)}, u32[]{:S(2)}) copy-start(bf16[2048,64]{0,1:T(8,128)(2,1)} %param.12) | copy-start | bytes 786436
  0.0 1.7 %copy-start.4 = (bf16[2048,64]{0,1:T(8,128)(2,1)S(1)}, bf16[2048,64]{0,1:T(8,128)(2,1)}, u32[]{:S(2)}) copy-start(bf16[2048,64]{0,1:T(8,128)(2,1)} %param.11) | copy-start | bytes 786436
  0.0 5.6 %copy-start.6 = (s32[1,8,8]{2,1,0:T(8,128)S(1)}, s32[1,8,8]{2,1,0:T(8,128)}, u32[]{:S(2)}) copy-start(s32[1,8,8]{2,1,0:T(8,128)} %refs_0_.1) | copy-start | bytes 772
  0.0 9.7 %copy-start.3 = (bf16[2048,256]{1,0:T(8,128)(2,1)S(1)}, bf16[2048,256]{1,0:T(8,128)(2,1)}, u32[]{:S(2)}) copy-start(bf16[2048,256]{1,0:T(8,128)(2,1)} %wq_ref.1) | copy-start | bytes 3145732
  2.6 11.1 %collective-permute-start.3 = (bf16[512,128]{1,0:T(8,128)(2,1)S(1)}, bf16[512,128]{1,0:T(8,128)(2,1)S(1)}, u32[]{:S(2)}, u32[]{:S(2)}) collective-permute-start(bf16[512,128]{1,0:T(8,128)(2,1)S(1)} %shard_map.93.pair_ref.refs_4_), channel_id=1, source_target_pairs={{0,4},{4,0},{8,12},{12,8},{16,20},{20,16},{24,28},{28,24},{1,5},{5... | collective-permute-start | bytes 393224 | tf_op jit(solution)/shard_map/ppermute | solution.py:322
  5.6 5.1 %collective-permute-start.1 = (s32[1,8,8]{2,1,0:T(8,128)S(1)}, s32[1,8,8]{2,1,0:T(8,128)S(1)}, u32[]{:S(2)}, u32[]{:S(2)}) collective-permute-start(s32[1,8,8]{2,1,0:T(8,128)S(1)} %copy-done.6), channel_id=1, source_target_pairs={{0,16},{4,20},{8,24},{12,28},{16,0},{20,4},{24,8},{28,12},{1,17},{... | collective-permute-start | bytes 776 | tf_op jit(solution)/shard_map/ppermute | solution.py:321
  8.2 5.4 %collective-permute-start = (s32[1,8,8]{2,1,0:T(8,128)S(1)}, s32[1,8,8]{2,1,0:T(8,128)S(1)}, u32[]{:S(2)}, u32[]{:S(2)}) collective-permute-start(s32[1,8,8]{2,1,0:T(8,128)S(1)} %copy-done.6), channel_id=1, source_target_pairs={{0,24},{4,28},{8,16},{12,20},{16,8},{20,12},{24,0},{28,4},{1,25},{... | collective-permute-start | bytes 776 | tf_op jit(solution)/shard_map/ppermute | solution.py:321
  9.6 4.1 %collective-permute-start.2 = (s32[1,8,8]{2,1,0:T(8,128)S(1)}, s32[1,8,8]{2,1,0:T(8,128)S(1)}, u32[]{:S(2)}, u32[]{:S(2)}) collective-permute-start(s32[1,8,8]{2,1,0:T(8,128)S(1)} %copy-done.6), channel_id=1, source_target_pairs={{0,8},{4,12},{8,0},{12,4},{16,24},{20,28},{24,16},{28,20},{1,9},{5... | collective-permute-start | bytes 776 | tf_op jit(solution)/shard_map/ppermute | solution.py:321
  13.8 6.1 %collective-permute-start.4 = (bf16[128,128]{1,0:T(8,128)(2,1)S(1)}, bf16[128,128]{1,0:T(8,128)(2,1)S(1)}, u32[]{:S(2)}, u32[]{:S(2)}) collective-permute-start(bf16[128,128]{1,0:T(8,128)(2,1)S(1)} %get-tuple-element.14), channel_id=1, source_target_pairs={{0,24},{4,28},{8,16},{12,20},{16,8},{20,12},{24,0},{28,4},{1,25},{... | collective-permute-start | bytes 98312 | tf_op jit(solution)/shard_map/ppermute | solution.py:332
  15.9 4.8 %collective-permute-start.5 = (bf16[128,128]{1,0:T(8,128)(2,1)S(1)}, bf16[128,128]{1,0:T(8,128)(2,1)S(1)}, u32[]{:S(2)}, u32[]{:S(2)}) collective-permute-start(bf16[128,128]{1,0:T(8,128)(2,1)S(1)} %get-tuple-element.15), channel_id=1, source_target_pairs={{0,16},{4,20},{8,24},{12,28},{16,0},{20,4},{24,8},{28,12},{1,17},{... | collective-permute-start | bytes 98312 | tf_op jit(solution)/shard_map/ppermute | solution.py:332
  15.9 4.8 %collective-permute-start.6 = (bf16[128,128]{1,0:T(8,128)(2,1)S(1)}, bf16[128,128]{1,0:T(8,128)(2,1)S(1)}, u32[]{:S(2)}, u32[]{:S(2)}) collective-permute-start(bf16[128,128]{1,0:T(8,128)(2,1)S(1)} %get-tuple-element.16), channel_id=1, source_target_pairs={{0,8},{4,12},{8,0},{12,4},{16,24},{20,28},{24,16},{28,20},{1,9},{5... | collective-permute-start | bytes 98312 | tf_op jit(solution)/shard_map/ppermute | solution.py:332
  20.0 7.9 %copy-start.1 = (bf16[1024,512]{1,0:T(8,128)(2,1)S(1)}, bf16[1024,512]{1,0:T(8,128)(2,1)}, u32[]{:S(2)}) copy-start(bf16[1024,512]{1,0:T(8,128)(2,1)} %refs_5_.3) | copy-start | bytes 3145732
  20.0 7.9 %copy-start.7 = (f32[1024]{0:T(1024)S(1)}, f32[1024]{0:T(1024)}, u32[]{:S(2)}) copy-start(f32[1024]{0:T(1024)} %param.14) | copy-start | bytes 12292
  21.0 5.0 %collective-permute-start.10 = (bf16[256,256]{1,0:T(8,128)(2,1)S(1)}, bf16[256,256]{1,0:T(8,128)(2,1)S(1)}, u32[]{:S(2)}, u32[]{:S(2)}) collective-permute-start(bf16[256,256]{1,0:T(8,128)(2,1)S(1)} %shard_map.97.refs_0_), channel_id=1, source_target_pairs={{0,2},{1,3},{2,0},{3,1},{4,6},{5,7},{6,4},{7,5},{8,10},{9,11},{10,... | collective-permute-start | bytes 393224 | tf_op jit(solution)/shard_map/ppermute | solution.py:366
  22.8 5.0 %collective-permute-start.7 = (bf16[256,256]{1,0:T(8,128)(2,1)S(1)}, bf16[256,256]{1,0:T(8,128)(2,1)S(1)}, u32[]{:S(2)}, u32[]{:S(2)}) collective-permute-start(bf16[256,256]{1,0:T(8,128)(2,1)S(1)} %shard_map.96.refs_0_), channel_id=1, source_target_pairs={{0,2},{1,3},{2,0},{3,1},{4,6},{5,7},{6,4},{7,5},{8,10},{9,11},{10,... | collective-permute-start | bytes 393224 | tf_op jit(solution)/shard_map/ppermute | solution.py:366
  23.4 4.4 %collective-permute-start.11 = (bf16[256,256]{1,0:T(8,128)(2,1)S(1)}, bf16[256,256]{1,0:T(8,128)(2,1)S(1)}, u32[]{:S(2)}, u32[]{:S(2)}) collective-permute-start(bf16[256,256]{1,0:T(8,128)(2,1)S(1)} %shard_map.97.refs_0_), channel_id=1, source_target_pairs={{0,1},{1,0},{2,3},{3,2},{4,5},{5,4},{6,7},{7,6},{8,9},{9,8},{10,11... | collective-permute-start | bytes 393224 | tf_op jit(solution)/shard_map/ppermute | solution.py:373
  26.0 1.8 %collective-permute-start.12 = (bf16[256,256]{1,0:T(8,128)(2,1)S(1)}, bf16[256,256]{1,0:T(8,128)(2,1)S(1)}, u32[]{:S(2)}, u32[]{:S(2)}) collective-permute-start(bf16[256,256]{1,0:T(8,128)(2,1)S(1)} %collective-permute-done.10.refs_1_), channel_id=1, source_target_pairs={{0,1},{1,0},{2,3},{3,2},{4,5},{5,4},{6,7},{7,6},{8,9},{9,8},{10,11... | collective-permute-start | bytes 393224 | tf_op jit(solution)/shard_map/ppermute | solution.py:373
  26.0 3.0 %collective-permute-start.8 = (bf16[256,256]{1,0:T(8,128)(2,1)S(1)}, bf16[256,256]{1,0:T(8,128)(2,1)S(1)}, u32[]{:S(2)}, u32[]{:S(2)}) collective-permute-start(bf16[256,256]{1,0:T(8,128)(2,1)S(1)} %shard_map.96.refs_0_), channel_id=1, source_target_pairs={{0,1},{1,0},{2,3},{3,2},{4,5},{5,4},{6,7},{7,6},{8,9},{9,8},{10,11... | collective-permute-start | bytes 393224 | tf_op jit(solution)/shard_map/ppermute | solution.py:373
  27.8 1.3 %collective-permute-start.9 = (bf16[256,256]{1,0:T(8,128)(2,1)S(1)}, bf16[256,256]{1,0:T(8,128)(2,1)S(1)}, u32[]{:S(2)}, u32[]{:S(2)}) collective-permute-start(bf16[256,256]{1,0:T(8,128)(2,1)S(1)} %collective-permute-done.7.refs_1_), channel_id=1, source_target_pairs={{0,1},{1,0},{2,3},{3,2},{4,5},{5,4},{6,7},{7,6},{8,9},{9,8},{10,11... | collective-permute-start | bytes 393224 | tf_op jit(solution)/shard_map/ppermute | solution.py:373
